TPU v7x, 512 devices: a whole 4x8x8 slice. The times are simulated.
512 devices in a mesh: ep: 128 (over z, y, core), tp: 4 (over x).
Axes of the slice: x: 4, y: 8, z: 8, core: 2. Of those that a mesh axis runs over, the one named last changes fastest.
Arguments:
- tokens: bfloat16 [2048, 1024], P(('ep', 'tp')), may hold values from -6 to 6
- lengths: int32 [2048], P('ep'), may hold values from 256 to 1024
- key_cache: bfloat16 [2048, 1024, 128], P(('ep', 'tp')), may hold values from -1500 to 1500
- value_cache: bfloat16 [2048, 1024, 128], P(('ep', 'tp')), may hold values from -6 to 6
- query_weight: bfloat16 [1024, 512], P(None, 'tp'), may hold values from -0.1875 to 0.1875
- key_weight: bfloat16 [1024, 128], replicated, may hold values from -0.1875 to 0.1875
- value_weight: bfloat16 [1024, 128], replicated, may hold values from -0.1875 to 0.1875
- lambdas: float32 [4], replicated, may hold values from 0.3 to 0.8
- head_gain: float32 [128], replicated, may hold values from 0.1 to 1.9
- output_weight: bfloat16 [512, 1024], P(None, 'tp'), may hold values from -0.25 to 0.25
- norm1_gain: float32 [1024], replicated, may hold values from 0.1 to 1.9
- routes: int32 [2048, 6], P('ep'), may hold values from 0 to 127, all different within a row; in each aligned block of 16 rows (0 to 15, 16 to 31, ...) at most 2 rows name the same one
- route_logits: float32 [2048, 6], P('ep'), may hold values from -9 to 410
- gate_weight: bfloat16 [128, 1024, 1024], P('ep', None, 'tp'), may hold values from -0.5 to 0.5
- up_weight: bfloat16 [128, 1024, 1024], P('ep', None, 'tp'), may hold values from -0.5 to 0.5
- down_weight: bfloat16 [128, 1024, 1024], P('ep', 'tp'), may hold values from -0.09375 to 0.09375
- norm2_gain: float32 [1024], replicated, may hold values from 0.1 to 1.9
Outputs:
- mixed: bfloat16 [2048, 1024], P('ep', 'tp')
Inputs may be any that keep to these rules, and one draw needn't show every extreme that they name: `routes`: in the 16 rows of each aligned block (the rows held by one index of ep) no expert is named by more than 2 rows, a bound that some block reaches; the experts of a row differ.
All inputs are finite; a program needn't handle non-finite values.
Results may differ from a plain program's by a relative error of at most 0.014.
Values may be sent and summed in bfloat16 or wider, within the bound.
A program may use at most 64 MiB of HBM per device.

v0:
```python
import jax
import jax.numpy as jnp
from jax import lax
from jax.sharding import PartitionSpec as P

ALPHA = 1.4142135623730951
EPS = 1e-05
THETA = 500000.0
LIMIT = 7.0
SLOPE = 1.702


def copy_for_each(x, axis):
    count = lax.axis_size(axis)
    return lax.all_to_all(jnp.broadcast_to(x[None], (count, *x.shape)), axis, 0, 0, tiled=True)


def in_order(pieces, dim):
    lengths = list(pieces.shape[1:])
    lengths[dim] *= pieces.shape[0]
    return jnp.moveaxis(pieces, 0, dim).reshape(lengths)


def gathered_copies(x, axis, dim):
    pieces = copy_for_each(x, axis)
    return in_order(pieces, dim)


def split_up(x, dim, count):
    lengths = x.shape
    pieces = x.reshape(*lengths[:dim], count, lengths[dim] // count, *lengths[dim + 1 :])
    return jnp.moveaxis(pieces, dim, 0)


def sum_at_owner(x, axis, dim):
    pieces = split_up(x, dim, lax.axis_size(axis))
    arrived = lax.all_to_all(pieces, axis, split_axis=0, concat_axis=0, tiled=True)
    return arrived.astype(jnp.float32).sum(axis=0)


def over_copies(x, axis):
    everything = copy_for_each(x, axis)
    return jnp.sum(everything, axis=0)


def packed_total(arrays, axis):
    ends = [0]
    for a in arrays:
        ends.append(ends[-1] + a.size)
    subtotal = over_copies(jnp.concatenate([a.ravel() for a in arrays]), axis)
    return tuple((subtotal[b:e].reshape(a.shape) for a, b, e in zip(arrays, ends, ends[1:])))


def rotate(values, positions):
    half = values.shape[-1] // 2
    freqs = THETA ** (-jnp.arange(half, dtype=jnp.float32) / half)
    angles = positions.astype(jnp.float32)[:, None] * freqs[None, :]
    shape = (angles.shape[0],) + (1,) * (values.ndim - 2) + (half,)
    cosine = jnp.cos(angles).reshape(shape)
    sine = jnp.sin(angles).reshape(shape)
    first = values[..., :half]
    second = values[..., half:]
    return jnp.concatenate(
        [first * cosine - second * sine, second * cosine + first * sine], axis=-1
    )


def norm_rows(summed, gain):
    mean = jnp.mean(summed, axis=-1, keepdims=True)
    center = summed - mean
    spread = jnp.mean(center * center, axis=-1, keepdims=True)
    return center * lax.rsqrt(spread + EPS) * gain


def scaled_part(summed, sums, squares, width, gain):
    mean = sums / width
    spread = squares / width - mean * mean
    return (summed - mean[:, None]) * lax.rsqrt(spread + EPS)[:, None] * gain


def choose_slots(routes_block, experts, capacity):
    flat = routes_block.reshape(-1)
    onehot = (flat[:, None] == jnp.arange(experts, dtype=jnp.int32)[None, :]).astype(jnp.int32)
    before = jnp.cumsum(onehot, axis=0) - onehot
    slot = jnp.sum(before * onehot, axis=1)
    target = flat * capacity + slot
    return target[:, None] == jnp.arange(experts * capacity, dtype=jnp.int32)[None, :]


def body(
    tokens,
    lengths,
    key_cache,
    value_cache,
    query_weight,
    key_weight,
    value_weight,
    lambdas,
    head_gain,
    output_weight,
    norm1_gain,
    routes,
    route_logits,
    gate_weight,
    up_weight,
    down_weight,
    norm2_gain,
):
    bf16 = jnp.bfloat16
    f32 = jnp.float32
    tp_count = lax.axis_size("tp")
    tp_rank = lax.axis_index("tp")
    own, width = tokens.shape
    group = own * tp_count
    part = width // tp_count
    heads = lambdas.shape[0]
    head_dim = key_weight.shape[1] // 2
    length = key_cache.shape[1]
    group_rows = gathered_copies(tokens, "tp", 0)
    query = jnp.dot(group_rows, query_weight, preferred_element_type=f32).reshape(
        group, -1, 2, head_dim
    )
    query = rotate(query, lengths).astype(bf16).reshape(group, -1)
    query = lax.all_to_all(query, "tp", split_axis=0, concat_axis=1, tiled=True).reshape(
        own, heads, 2, head_dim
    )
    own_lengths = lax.dynamic_slice_in_dim(lengths, tp_rank * own, own)
    new_key = jnp.dot(tokens, key_weight, preferred_element_type=f32).reshape(own, 2, head_dim)
    new_key = rotate(new_key, own_lengths).astype(bf16)
    new_value = jnp.dot(tokens, value_weight, preferred_element_type=f32).astype(bf16)
    keys = key_cache.reshape(own, length, 2, head_dim)
    scale = head_dim ** (-0.5)
    past = jnp.einsum("bhmd,bjmd->bhmj", query, keys, preferred_element_type=f32) * scale
    live = jnp.arange(length, dtype=jnp.int32)[None, :] < own_lengths[:, None]
    past = jnp.where(live[:, None, None, :], past, -jnp.inf)
    selfs = jnp.einsum("bhmd,bmd->bhm", query, new_key, preferred_element_type=f32) * scale
    top = jnp.maximum(jnp.max(past, axis=-1), selfs)
    past_exp = jnp.exp(past - top[..., None])
    self_exp = jnp.exp(selfs - top)
    total = jnp.sum(past_exp, axis=-1) + self_exp
    past_prob = past_exp / total[..., None]
    self_prob = self_exp / total
    mixing = lambdas[None, :]
    past_weight = (past_prob[:, :, 0] - mixing[..., None] * past_prob[:, :, 1]).astype(bf16)
    self_weight = (self_prob[:, :, 0] - mixing * self_prob[:, :, 1]).astype(bf16)
    head_out = jnp.einsum("bhj,bje->bhe", past_weight, value_cache, preferred_element_type=f32)
    head_out = head_out + self_weight.astype(f32)[..., None] * new_value.astype(f32)[:, None, :]
    normed = (
        head_out
        * lax.rsqrt(jnp.mean(head_out * head_out, axis=-1, keepdims=True) + EPS)
        * head_gain
    )
    attended = normed.astype(bf16).reshape(own, -1)
    mix = jnp.dot(gathered_copies(attended, "tp", 0), output_weight, preferred_element_type=f32)
    column_start = tp_rank * part
    own_columns = lax.dynamic_slice_in_dim(group_rows, column_start, part, 1).astype(f32)
    summed = ALPHA * own_columns + mix
    whole = gathered_copies(summed, "tp", 1)
    settled = norm_rows(whole, norm1_gain).astype(bf16)
    settled_part = lax.dynamic_slice_in_dim(settled, column_start, part, 1)
    experts = lax.axis_size("ep")
    topk = routes.shape[1]
    capacity = min(group, max(2, 2 * group * topk // experts))
    chosen = choose_slots(routes, experts, capacity)
    placing = jnp.sum(chosen.reshape(group, topk, -1).astype(f32), axis=1).astype(bf16)
    route_weight = jax.nn.softmax(route_logits, axis=-1)
    gate_local = gate_weight[0]
    up_local = up_weight[0]
    down_local = down_weight[0]
    outgoing = lax.dot_general(
        placing, settled, (((0,), (0,)), ((), ())), preferred_element_type=f32
    )
    outgoing = outgoing.astype(bf16).reshape(experts, capacity, width)
    rows = lax.all_to_all(outgoing, "ep", split_axis=0, concat_axis=0, tiled=True)
    gate_h = jnp.einsum("scd,df->scf", rows, gate_local, preferred_element_type=f32)
    up_h = jnp.einsum("scd,df->scf", rows, up_local, preferred_element_type=f32)
    clipped = jnp.minimum(gate_h, LIMIT)
    linear = jnp.clip(up_h, -LIMIT, LIMIT)
    act = (clipped * jax.nn.sigmoid(SLOPE * clipped) * (linear + 1.0)).astype(bf16)
    terms = jnp.einsum("scf,fd->scd", act, down_local, preferred_element_type=f32)
    answers = sum_at_owner(terms.astype(jnp.bfloat16), "tp", 2).astype(bf16)
    selector = chosen.astype(bf16)
    back = lax.all_to_all(answers, "ep", split_axis=0, concat_axis=0, tiled=True)
    picked = jnp.dot(selector, back.reshape(experts * capacity, -1), preferred_element_type=f32)
    routed = jnp.sum(picked.reshape(group, topk, -1) * route_weight[:, :, None], axis=1)
    final = ALPHA * settled_part.astype(f32) + routed
    sums, squares = packed_total((jnp.sum(final, axis=1), jnp.sum(final * final, axis=1)), "tp")
    gain_part = lax.dynamic_slice_in_dim(norm2_gain, column_start, part)
    result = scaled_part(final, sums, squares, width, gain_part).astype(bf16)
    return result


def solution(mesh):
    in_specs = (
        P(("ep", "tp"), None),
        P("ep"),
        P(("ep", "tp"), None, None),
        P(("ep", "tp"), None, None),
        P(None, "tp"),
        P(),
        P(),
        P(),
        P(),
        P(None, "tp"),
        P(),
        P("ep", None),
        P("ep", None),
        P("ep", None, "tp"),
        P("ep", None, "tp"),
        P("ep", "tp", None),
        P(),
    )
    out_specs = P("ep", "tp")
    return jax.shard_map(body, mesh=mesh, in_specs=in_specs, out_specs=out_specs, check_vma=False)
```

profile of v0, /device:TPU:1, one launch (start us, length us, event | category | flops | bytes accessed | tf_op | source)
XLA Modules:
  0.0 130.2 jit_solution(14348994020305583358)
XLA Ops:
  0.0 1.5 %broadcast_in_dim.22 = bf16[4,4,1024]{2,1,0:T(4,128)(2,1)} broadcast(bf16[4,1024]{1,0:T(4,128)(2,1)} %param.17), dimensions={1,2} | broadcast | bytes 40960 | tf_op jit(solution)/shard_map/broadcast_in_dim | solution.py:15
  1.5 4.8 %all-to-all-start = ((bf16[4,4,1024]{2,1,0:T(4,128)(2,1)}), bf16[4,4,1024]{2,1,0:T(4,128)(2,1)S(1)}, u32[]{:S(2)}, u32[]{:S(2)}) async-start(bf16[4,4,1024]{2,1,0:T(4,128)(2,1)} %broadcast_in_dim.22), calls=%async_computation | async-start | bytes 65536 | tf_op jit(solution)/shard_map/all_to_all | solution.py:15
  6.3 0.7 convert_element_type.67
  7.0 0.7 fusion.54
  7.7 1.1 fusion.56
  9.2 0.8 fusion.6
  10.1 0.8 copy.109
  11.4 1.1 copy.102
  12.9 0.7 convert_element_type.68
  13.6 4.2 %all-to-all-start.1 = ((bf16[4,4,128]{2,1,0:T(4,128)(2,1)}), bf16[4,4,128]{2,1,0:T(4,128)(2,1)S(1)}, u32[]{:S(2)}, u32[]{:S(2)}) async-start(bf16[4,4,128]{2,1,0:T(4,128)(2,1)} %convert_element_type.68), calls=%async_computation.1 | async-start | bytes 8192 | tf_op jit(solution)/shard_map/all_to_all | solution.py:124
  18.6 3.4 %all-to-all-done.1 = bf16[4,4,128]{2,1,0:T(4,128)(2,1)S(1)} async-done(((bf16[4,4,128]{2,1,0:T(4,128)(2,1)}), bf16[4,4,128]{2,1,0:T(4,128)(2,1)S(1)}, u32[]{:S(2)}, u32[]{:S(2)}) %all-to-all-start.1) | async-done | bytes 4128 | tf_op jit(solution)/shard_map/all_to_all | solution.py:124
  22.9 0.6 copy-done.7
  24.0 0.7 copy-done.8
  25.4 3.4 %all-to-all-start.2 = ((bf16[4,4,512]{2,1,0:T(4,128)(2,1)}), bf16[4,4,512]{2,1,0:T(4,128)(2,1)S(1)}, u32[]{:S(2)}, u32[]{:S(2)}) async-start(bf16[4,4,512]{2,1,0:T(4,128)(2,1)} %broadcast_in_dim.26), calls=%async_computation.2 | async-start | bytes 32768 | tf_op jit(solution)/shard_map/all_to_all | solution.py:15
  28.8 4.1 %all-to-all-done.2 = bf16[4,4,512]{2,1,0:T(4,128)(2,1)S(1)} async-done(((bf16[4,4,512]{2,1,0:T(4,128)(2,1)}), bf16[4,4,512]{2,1,0:T(4,128)(2,1)S(1)}, u32[]{:S(2)}, u32[]{:S(2)}) %all-to-all-start.2) | async-done | bytes 16416 | tf_op jit(solution)/shard_map/all_to_all | solution.py:15
  33.1 0.6 broadcast_in_dim.27
  33.7 3.3 %all-to-all-start.3 = ((f32[4,16,256]{2,1,0:T(8,128)}), f32[4,16,256]{2,1,0:T(8,128)S(1)}, u32[]{:S(2)}, u32[]{:S(2)}) async-start(f32[4,16,256]{2,1,0:T(8,128)} %broadcast_in_dim.27), calls=%async_computation.3 | async-start | bytes 131072 | tf_op jit(solution)/shard_map/all_to_all | solution.py:15
  37.1 4.4 %all-to-all-done.3 = f32[4,16,256]{2,1,0:T(8,128)S(1)} async-done(((f32[4,16,256]{2,1,0:T(8,128)}), f32[4,16,256]{2,1,0:T(8,128)S(1)}, u32[]{:S(2)}, u32[]{:S(2)}) %all-to-all-start.3) | async-done | bytes 65568 | tf_op jit(solution)/shard_map/all_to_all | solution.py:15
  41.8 0.7 copy-done.6
  43.1 42.4 %all_to_all.49 = bf16[128,2,1024]{2,1,0:T(2,128)(2,1)S(1)} all-to-all(bf16[128,2,1024]{2,1,0:T(2,128)(2,1)S(1)} %reshape.272), channel_id=1, replica_groups=mesh['ep'=128,'tp'=4] {'ep'}, dimensions={0} | all-to-all | bytes 1048576 | tf_op jit(solution)/shard_map/all_to_all | solution.py:174
  85.8 0.7 copy-done.10
  86.7 0.7 convolution_convert_fusion
  87.4 0.8 copy.141
  88.2 3.6 %all-to-all-start.5 = ((bf16[4,128,2,256]{3,1,2,0:T(8,128)(2,1)}), bf16[4,128,2,256]{3,1,2,0:T(8,128)(2,1)S(1)}, u32[]{:S(2)}, u32[]{:S(2)}) async-start(bf16[4,128,2,256]{3,1,2,0:T(8,128)(2,1)} %bitcast.101), calls=%async_computation.5 | async-start | bytes 1048576 | tf_op jit(solution)/shard_map/all_to_all | solution.py:37
  91.9 9.8 %all-to-all-done.5 = bf16[4,128,2,256]{3,1,2,0:T(8,128)(2,1)S(1)} async-done(((bf16[4,128,2,256]{3,1,2,0:T(8,128)(2,1)}), bf16[4,128,2,256]{3,1,2,0:T(8,128)(2,1)S(1)}, u32[]{:S(2)}, u32[]{:S(2)}) %all-to-all-start.5) | async-done | bytes 524320 | tf_op jit(solution)/shard_map/all_to_all | solution.py:37
  101.7 0.8 copy.115
  102.5 5.8 %all-to-all-start.6 = ((bf16[128,2,256]{2,1,0:T(2,128)(2,1)}), bf16[128,2,256]{2,1,0:T(2,128)(2,1)S(1)}, u32[]{:S(2)}, u32[]{:S(2)}) async-start(bf16[128,2,256]{2,1,0:T(2,128)(2,1)} %copy.115), calls=%async_computation.6 | async-start | bytes 262144 | tf_op jit(solution)/shard_map/all_to_all | solution.py:183
  108.3 12.8 %all-to-all-done.6 = bf16[128,2,256]{2,1,0:T(2,128)(2,1)S(1)} async-done(((bf16[128,2,256]{2,1,0:T(2,128)(2,1)}), bf16[128,2,256]{2,1,0:T(2,128)(2,1)S(1)}, u32[]{:S(2)}, u32[]{:S(2)}) %all-to-all-start.6) | async-done | bytes 131104 | tf_op jit(solution)/shard_map/all_to_all | solution.py:183
  122.2 3.2 %all-to-all-start.7 = ((f32[4,1,32]{2,1,0:T(1,128)}), f32[4,1,32]{2,1,0:T(1,128)S(1)}, u32[]{:S(2)}, u32[]{:S(2)}) async-start(f32[4,1,32]{2,1,0:T(1,128)} %broadcast_in_dim.28), calls=%async_computation.7 | async-start | bytes 4096 | tf_op jit(solution)/shard_map/all_to_all | solution.py:15
  125.4 0.8 dynamic_slice.15
  126.2 3.3 %all-to-all-done.7 = f32[4,1,32]{2,1,0:T(1,128)S(1)} async-done(((f32[4,1,32]{2,1,0:T(1,128)}), f32[4,1,32]{2,1,0:T(1,128)S(1)}, u32[]{:S(2)}, u32[]{:S(2)}) %all-to-all-start.7) | async-done | bytes 544 | tf_op jit(solution)/shard_map/all_to_all | solution.py:15
  129.5 0.7 multiply_convert_fusion.1
  (78 shorter events, 7.1 us)
Async XLA Ops:
  0.0 23.6 %copy-start = (bf16[4,1024,128]{2,1,0:T(8,128)(2,1)S(1)}, bf16[4,1024,128]{2,1,0:T(8,128)(2,1)}, u32[]{:S(2)}) copy-start(bf16[4,1024,128]{2,1,0:T(8,128)(2,1)} %param.20) | copy-start | bytes 3145732
  0.0 9.2 %copy-start.3 = (bf16[1024,128]{1,0:T(8,128)(2,1)S(1)}, bf16[1024,128]{1,0:T(8,128)(2,1)}, u32[]{:S(2)}) copy-start(bf16[1024,128]{1,0:T(8,128)(2,1)} %param.23) | copy-start | bytes 786436
  0.0 17.9 %copy-start.1 = (bf16[4,1024,128]{2,1,0:T(8,128)(2,1)S(1)}, bf16[4,1024,128]{2,1,0:T(8,128)(2,1)}, u32[]{:S(2)}) copy-start(bf16[4,1024,128]{2,1,0:T(8,128)(2,1)} %param.19) | copy-start | bytes 3145732
  1.5 11.0 %all-to-all-start = ((bf16[4,4,1024]{2,1,0:T(4,128)(2,1)}), bf16[4,4,1024]{2,1,0:T(4,128)(2,1)S(1)}, u32[]{:S(2)}, u32[]{:S(2)}) async-start(bf16[4,4,1024]{2,1,0:T(4,128)(2,1)} %broadcast_in_dim.22), calls=%async_computation | async-start | bytes 65536 | tf_op jit(solution)/shard_map/all_to_all | solution.py:15
  13.6 8.4 %all-to-all-start.1 = ((bf16[4,4,128]{2,1,0:T(4,128)(2,1)}), bf16[4,4,128]{2,1,0:T(4,128)(2,1)S(1)}, u32[]{:S(2)}, u32[]{:S(2)}) async-start(bf16[4,4,128]{2,1,0:T(4,128)(2,1)} %convert_element_type.68), calls=%async_computation.1 | async-start | bytes 8192 | tf_op jit(solution)/shard_map/all_to_all | solution.py:124
  22.9 0.7 copy-start.7
  23.6 9.3 %copy-start.2 = (bf16[512,256]{1,0:T(8,128)(2,1)S(1)}, bf16[512,256]{1,0:T(8,128)(2,1)}, u32[]{:S(2)}) copy-start(bf16[512,256]{1,0:T(8,128)(2,1)} %param.26) | copy-start | bytes 786436
  24.0 0.7 copy-start.8
  25.3 3.4 %copy-start.5 = (s32[16,6]{0,1:T(8,128)S(1)}, s32[16,6]{0,1:T(8,128)}, u32[]{:S(2)}) copy-start(s32[16,6]{0,1:T(8,128)} %param.28) | copy-start | bytes 1156
  25.4 7.6 %all-to-all-start.2 = ((bf16[4,4,512]{2,1,0:T(4,128)(2,1)}), bf16[4,4,512]{2,1,0:T(4,128)(2,1)S(1)}, u32[]{:S(2)}, u32[]{:S(2)}) async-start(bf16[4,4,512]{2,1,0:T(4,128)(2,1)} %broadcast_in_dim.26), calls=%async_computation.2 | async-start | bytes 32768 | tf_op jit(solution)/shard_map/all_to_all | solution.py:15
  33.7 7.7 %all-to-all-start.3 = ((f32[4,16,256]{2,1,0:T(8,128)}), f32[4,16,256]{2,1,0:T(8,128)S(1)}, u32[]{:S(2)}, u32[]{:S(2)}) async-start(f32[4,16,256]{2,1,0:T(8,128)} %broadcast_in_dim.27), calls=%async_computation.3 | async-start | bytes 131072 | tf_op jit(solution)/shard_map/all_to_all | solution.py:15
  41.8 0.7 copy-start.6
  43.1 42.4 %copy-start.9 = (bf16[1,1024,256]{2,1,0:T(8,128)(2,1)S(1)}, bf16[1,1024,256]{2,1,0:T(8,128)(2,1)}, u32[]{:S(2)}) copy-start(bf16[1,1024,256]{2,1,0:T(8,128)(2,1)} %param.30) | copy-start | bytes 1572868
  85.5 1.0 copy-start.10
  85.5 1.2 copy-start.11
  88.2 3.6 %copy-start.4 = (f32[16,6]{0,1:T(8,128)S(1)}, f32[16,6]{0,1:T(8,128)}, u32[]{:S(2)}) copy-start(f32[16,6]{0,1:T(8,128)} %param.29) | copy-start | bytes 1156
  88.2 13.4 %all-to-all-start.5 = ((bf16[4,128,2,256]{3,1,2,0:T(8,128)(2,1)}), bf16[4,128,2,256]{3,1,2,0:T(8,128)(2,1)S(1)}, u32[]{:S(2)}, u32[]{:S(2)}) async-start(bf16[4,128,2,256]{3,1,2,0:T(8,128)(2,1)} %bitcast.101), calls=%async_computation.5 | async-start | bytes 1048576 | tf_op jit(solution)/shard_map/all_to_all | solution.py:37
  102.5 18.6 %all-to-all-start.6 = ((bf16[128,2,256]{2,1,0:T(2,128)(2,1)}), bf16[128,2,256]{2,1,0:T(2,128)(2,1)S(1)}, u32[]{:S(2)}, u32[]{:S(2)}) async-start(bf16[128,2,256]{2,1,0:T(2,128)(2,1)} %copy.115), calls=%async_computation.6 | async-start | bytes 262144 | tf_op jit(solution)/shard_map/all_to_all | solution.py:183
  122.2 7.3 %all-to-all-start.7 = ((f32[4,1,32]{2,1,0:T(1,128)}), f32[4,1,32]{2,1,0:T(1,128)S(1)}, u32[]{:S(2)}, u32[]{:S(2)}) async-start(f32[4,1,32]{2,1,0:T(1,128)} %broadcast_in_dim.28), calls=%async_computation.7 | async-start | bytes 4096 | tf_op jit(solution)/shard_map/all_to_all | solution.py:15
where the time goes:
time: 131 us; the launch traced here: 130 us
  blocking collectives  42.4 us (32%)
  waiting for transfers between devices  37.7 us (29%)
  starting transfers between devices  28.3 us (22%)
  local copies, waits for them, and re-layouts  12.4 us (9%)
  matrix products  4.71 us (4%)
  other arithmetic  4.47 us (3%)
    all_to_all x1, blocking collectives, body(): lax.all_to_all(outgoing, 'ep', split_axis=0, concat_axis=0, tiled=True)  42.4 us
    all_to_all x4, starting transfers between devices, copy_for_each(): lax.all_to_all(jnp.broadcast_to(x[None], (count, *x.shape)), axis, 0, 0,...  14.7 us
    all_to_all x1, waiting for transfers between devices, body(): lax.all_to_all(answers, 'ep', split_axis=0, concat_axis=0, tiled=True)  12.8 us
    all_to_all x4, waiting for transfers between devices, copy_for_each(): lax.all_to_all(jnp.broadcast_to(x[None], (count, *x.shape)), axis, 0, 0,...  11.7 us
    all_to_all x1, waiting for transfers between devices, sum_at_owner(): lax.all_to_all(pieces, axis, split_axis=0, concat_axis=0, tiled=True)  9.76 us
    all_to_all x1, starting transfers between devices, body(): lax.all_to_all(answers, 'ep', split_axis=0, concat_axis=0, tiled=True)  5.77 us
    unnamed x28, local copies, waits for them, and re-layouts  5.31 us
    all_to_all x1, starting transfers between devices, body(): lax.all_to_all(query, 'tp', split_axis=0, concat_axis=1, tiled=True)  4.23 us
  transfers between devices with their start and end apart: 7, of which 6 were waited for; matrix products, arithmetic and copies ran while one was open for 6% of the time, Pallas kernels for 0%

commit v1 on v0

v1 whole, which is shorter than its diff:
```python
import functools

import jax
import jax.numpy as jnp
from jax import lax
from jax.experimental import pallas as pl
from jax.experimental.pallas import tpu as pltpu
from jax.sharding import PartitionSpec as P

ALPHA = 1.4142135623730951
EPS = 1e-05
THETA = 500000.0
LIMIT = 7.0
SLOPE = 1.702
LANES = 128
MESH = pl.DeviceIdType.MESH
BF16 = jnp.bfloat16
F32 = jnp.float32


def log2(n):
    return n.bit_length() - 1


def iota(shape, dim):
    return lax.broadcasted_iota(jnp.int32, shape, dim)


def ones_where(mask):
    return jnp.where(mask, 1.0, 0.0)


def dot(a, b):
    return jnp.dot(a, b, preferred_element_type=F32)


def zigzag(i, n):
    step = (i + 1) // 2
    return lax.rem(n // 2 + (1 - 2 * ((i + 1) % 2)) * step + n, n)


class Sizes:
    def __init__(self, nz, nyc, tp, own, blocks, heads, length, topk, cap):
        self.nz, self.nyc, self.tp, self.own = nz, nyc, tp, own
        self.blocks, self.heads, self.length = blocks, heads, length
        self.topk, self.cap = topk, cap
        self.group = own * tp
        self.rows = nz * nyc * cap
        self.zrows = nyc * cap
        self.yrows = nz * cap


class Exchange:
    def __init__(self, sizes, along_z, ep, out, into, send, recv):
        self.sizes, self.along_z, self.ep = sizes, along_z, ep
        self.out, self.into, self.send, self.recv = out, into, send, recv
        self.count = sizes.nz if along_z else sizes.nyc

    def peer(self, i):
        s = self.sizes
        z, yc = self.ep // s.nyc, self.ep % s.nyc
        if self.along_z:
            other = lax.rem(z + zigzag(i, s.nz), s.nz)
            return other, other * s.nyc + yc
        ny = s.nyc // 2
        y, c = yc // 2, yc % 2
        other = lax.rem(y + zigzag(i // 2, ny), ny) * 2 + lax.rem(c + 1 - i % 2, 2)
        return other, z * s.nyc + other

    def me(self):
        return self.ep // self.sizes.nyc if self.along_z else self.ep % self.sizes.nyc

    def copy(self, i):
        other, device = self.peer(i)
        return pltpu.make_async_remote_copy(
            src_ref=self.out.at[other],
            dst_ref=self.into.at[self.me()],
            send_sem=self.send.at[i],
            recv_sem=self.recv.at[i],
            device_id={"ep": device},
            device_id_type=MESH,
        )

    def loop(self, action):
        def step(i, carry):
            action(i)
            return carry

        lax.fori_loop(0, self.count - 1, step, 0)

    def start(self):
        self.loop(lambda i: self.copy(i).start())
        mine = self.me()
        self.into[mine] = self.out[mine]

    def wait_recv(self):
        self.loop(lambda i: self.copy(i).wait_recv())

    def wait_send(self):
        self.loop(lambda i: self.copy(i).wait_send())


def kernel(
    s,
    tok_ref,
    len_ref,
    cos_ref,
    sin_ref,
    routes_ref,
    routes_t_ref,
    logits_ref,
    lam_ref,
    hgain_ref,
    gain1_ref,
    gain2_ref,
    wq_hbm,
    wk_hbm,
    wv_hbm,
    wo_hbm,
    kc_hbm,
    vc_hbm,
    gate_hbm,
    up_hbm,
    down_hbm,
    out_ref,
    wq,
    wk,
    wv,
    wo,
    kc,
    vc,
    gate,
    up,
    down,
    tokbuf,
    xs,
    qbuf,
    nk_s,
    nv_s,
    attbuf,
    stats1,
    stats2,
    pzy,
    pyz,
    pla,
    plb,
    ca,
    cb,
    dz1o,
    dz1i,
    dy1o,
    dy1i,
    dy2o,
    dz2o,
    dz2i,
    xb,
    gacc,
    uacc,
    r2o,
    r2i,
    rdo,
    rdi,
    rpo,
    rpi,
    ey1o,
    ey1i,
    ez2o,
    ez2i,
    ez1o,
    ez1i,
    ey2o,
    ey2i,
    load_sem,
    tp_send,
    tp_recv,
    x_send,
    x_recv,
    z_send,
    z_recv,
    y_send,
    y_recv,
):
    ep = lax.axis_index("ep")
    t = lax.axis_index("tp")
    tp, own, group, heads = s.tp, s.own, s.group, s.heads
    rows, cap = s.rows, s.cap
    part = 2 * LANES
    nxt = lax.rem(t + 1, tp)
    far = lax.rem(t + 2, tp)
    prv = lax.rem(t + 3, tp)

    pairs = [
        (wq_hbm, wq),
        (wk_hbm, wk),
        (wv_hbm, wv),
        (kc_hbm, kc),
        (vc_hbm, vc),
        (wo_hbm, wo),
        (gate_hbm, gate),
        (up_hbm, up),
        (down_hbm, down),
    ]
    loads = [pltpu.make_async_copy(a, b, load_sem.at[i]) for i, (a, b) in enumerate(pairs)]

    barrier = pltpu.get_barrier_semaphore()
    probe_z = Exchange(s, True, ep, None, None, None, None)
    probe_y = Exchange(s, False, ep, None, None, None, None)

    def greet(device):
        pl.semaphore_signal(barrier, inc=1, device_id=device, device_id_type=MESH)

    probe_z.loop(lambda i: greet({"ep": probe_z.peer(i)[1]}))
    probe_y.loop(lambda i: greet({"ep": probe_y.peer(i)[1]}))
    for d in range(1, tp):
        greet({"tp": lax.rem(t + d, tp)})
    for load in loads:
        load.start()

    lc, lz = log2(cap), log2(s.nz)

    def slots(r, z_major):
        slot = r & (cap - 1)
        if z_major:
            return r >> lc, slot
        z = (r >> lc) & (s.nz - 1)
        return z * s.nyc + (r >> (lc + lz)), slot

    r0, c0 = iota((rows, rows), 0), iota((rows, rows), 1)
    lyc = log2(s.nyc)
    z_of, yc_of = (r0 >> lc) & (s.nz - 1), r0 >> (lc + lz)
    pzy[...] = ones_where(c0 == (z_of * s.nyc + yc_of) * cap + (r0 & (cap - 1))).astype(BF16)
    yc_of, z_of = (r0 >> lc) & (s.nyc - 1), r0 >> (lc + lyc)
    pyz[...] = ones_where(c0 == (yc_of * s.nz + z_of) * cap + (r0 & (cap - 1))).astype(BF16)

    logits = logits_ref[...]
    raised = jnp.exp(logits - jnp.max(logits, axis=-1, keepdims=True))
    route_weight = raised / jnp.sum(raised, axis=-1, keepdims=True)
    upper = ones_where(iota((group, group), 0) < iota((group, group), 1)).astype(BF16)
    lower = ones_where(iota((group, group), 1) < iota((group, group), 0)).astype(BF16)
    for z_major, pl_ref, c_ref in ((True, pla, ca), (False, plb, cb)):
        expert, slot = slots(iota((rows, group), 0), z_major)
        named = jnp.zeros((rows, group), F32)
        for k in range(s.topk):
            named += ones_where(routes_t_ref[k : k + 1, :] == expert)
        before = dot(named.astype(BF16), upper)
        pl_ref[...] = jnp.where(before == slot.astype(F32), named, 0.0).astype(BF16)
        expert, slot = slots(iota((group, rows), 1), z_major)
        named = jnp.zeros((group, rows), F32)
        weighed = jnp.zeros((group, rows), F32)
        for k in range(s.topk):
            hit = routes_ref[:, k : k + 1] == expert
            named += ones_where(hit)
            weighed += jnp.where(hit, route_weight[:, k : k + 1], 0.0)
        before = dot(lower, named.astype(BF16))
        weighed = jnp.where(before == slot.astype(F32), weighed, 0.0)
        for i in range(3):
            piece = weighed.astype(BF16)
            c_ref[i * group : (i + 1) * group, :] = piece
            weighed = weighed - piece.astype(F32)

    def tp_copies(phase, src, buf):
        return [
            pltpu.make_async_remote_copy(
                src_ref=src,
                dst_ref=buf.at[t],
                send_sem=tp_send.at[phase, d - 1],
                recv_sem=tp_recv.at[phase, d - 1],
                device_id={"tp": lax.rem(t + d, tp)},
                device_id_type=MESH,
            )
            for d in (2, 1, 3)
        ]

    sent = []

    def gather(phase, src, buf):
        copies = tp_copies(phase, src, buf)
        for copy in copies:
            copy.start()
        sent.extend(copies)
        return copies

    def arrived(copies):
        for copy in copies:
            copy.wait_recv()

    tokbuf[t] = tok_ref[...]
    pl.semaphore_wait(barrier, s.nz - 1 + s.nyc - 1 + tp - 1)

    copies = gather(0, tok_ref, tokbuf)
    nrow = tp * s.blocks * own
    r0, c0 = iota((nrow, nrow), 0), iota((nrow, nrow), 1)
    lo, lt, lb = log2(own), log2(tp), log2(s.blocks)
    origin = (((r0 >> lo) & (tp - 1)) << (lb + lo)) + ((r0 >> (lo + lt)) << lo) + (r0 & (own - 1))
    order = ones_where(c0 == origin).astype(BF16)
    loads[0].wait()
    arrived(copies)
    x = dot(order, tokbuf[...].reshape(nrow, LANES)).astype(BF16)
    xs[...] = x.reshape(s.blocks, group, LANES)
    x = jnp.concatenate([xs[i] for i in range(s.blocks)], axis=-1)

    cosine, sine = cos_ref[...], sin_ref[...]
    lane = iota((group, LANES), 1)

    def rotate(v):
        swapped = jnp.where((lane & 32) == 0, pltpu.roll(v, 96, 1), pltpu.roll(v, 32, 1))
        return (v * cosine + swapped * sine).astype(BF16)

    qbuf[t] = rotate(dot(x, wq[...]))
    copies = gather(1, qbuf.at[t], qbuf)
    loads[1].wait()
    loads[2].wait()
    nk_s[...] = rotate(dot(x, wk[...])).astype(F32)
    nv_s[...] = dot(x, wv[...]).astype(BF16).astype(F32)

    lh = log2(heads)
    nq = own * 2 * heads
    r0, c0 = iota((nq, heads * group), 0), iota((nq, heads * group), 1)
    source = ((r0 & (heads - 1)) * group) + t * own + (r0 >> (lh + 1))
    order = ones_where(c0 == source).astype(BF16)
    loads[3].wait()
    loads[4].wait()
    arrived(copies)
    q = dot(order, qbuf[...].reshape(heads * group, LANES))
    q = jnp.where((iota((nq, LANES), 1) >> 6) == ((iota((nq, LANES), 0) >> lh) & 1), q, 0.0)
    position = iota((2 * heads, s.length), 1)
    head = iota((2 * heads, 1), 0) & (heads - 1)
    lam = jnp.zeros((2 * heads, 1), F32)
    for h in range(heads):
        lam = jnp.where(head == h, lam_ref[h], lam)
    outs = []
    for b in range(own):
        qb = q[b * 2 * heads : (b + 1) * 2 * heads, :]
        score = lax.dot_general(
            qb.astype(BF16), kc[b], (((1,), (1,)), ((), ())), preferred_element_type=F32
        )
        score = jnp.where(position < len_ref[t * own + b], score * 0.125, -jnp.inf)
        own_score = jnp.sum(qb * nk_s[pl.ds(t * own + b, 1), :], axis=-1, keepdims=True) * 0.125
        top = jnp.maximum(jnp.max(score, axis=-1, keepdims=True), own_score)
        e = jnp.exp(score - top)
        e_own = jnp.exp(own_score - top)
        total = jnp.sum(e, axis=-1, keepdims=True) + e_own
        prob = e / total
        prob_own = jnp.broadcast_to(e_own / total, (2 * heads, LANES))
        weight = (prob - lam * pltpu.roll(prob, heads, 0)).astype(BF16)
        weight_own = (prob_own - lam * pltpu.roll(prob_own, heads, 0)).astype(BF16).astype(F32)
        ho = dot(weight, vc[b]) + weight_own * nv_s[pl.ds(t * own + b, 1), :]
        scale = lax.rsqrt(jnp.mean(ho * ho, axis=-1, keepdims=True) + EPS)
        outs.append(ho * scale * hgain_ref[...])
    attbuf[t] = jnp.concatenate(outs, axis=0).astype(BF16)

    copies = gather(2, attbuf.at[t], attbuf)
    r0, c0 = iota((heads * group, tp * nq), 0), iota((heads * group, tp * nq), 1)
    lg = log2(group)
    token = r0 & (group - 1)
    source = (token >> lo) * nq + (token & (own - 1)) * (2 * heads) + (r0 >> lg)
    order = ones_where(c0 == source).astype(BF16)
    loads[5].wait()
    columns = jnp.concatenate([xs[2 * t], xs[2 * t + 1]], axis=-1).astype(F32)
    arrived(copies)
    att = dot(order, attbuf[...].reshape(tp * nq, LANES)).astype(BF16)
    att = jnp.concatenate([att[h * group : (h + 1) * group, :] for h in range(heads)], axis=-1)
    summed = ALPHA * columns + dot(att, wo[...])

    def normed(v, phase, stats, gain):
        mean = jnp.mean(v, axis=-1, keepdims=True)
        center = v - mean
        square = jnp.sum(center * center, axis=-1, keepdims=True)
        stats[t] = jnp.where(lane == 0, mean, jnp.where(lane == 1, square, 0.0))
        arrived(gather(phase, stats.at[t], stats))
        means = [stats[i][:, 0:1] for i in range(tp)]
        squares = [stats[i][:, 1:2] for i in range(tp)]
        mean = sum(means) / tp
        spread = (sum(squares) + part * sum((m - mean) ** 2 for m in means)) / (tp * part)
        return ((v - mean) * lax.rsqrt(spread + EPS) * gain[pl.ds(t, 1), :]).astype(BF16)

    settled = normed(summed, 3, stats1, gain1_ref)

    nz, nyc, zrows, yrows = s.nz, s.nyc, s.zrows, s.yrows
    xmine = xb.at[t, 0]
    dza = Exchange(s, True, ep, dz1o, dz1i, z_send.at[0], z_recv.at[0])
    dyb = Exchange(s, False, ep, dy1o, dy1i, y_send.at[0], y_recv.at[0])
    dya = Exchange(s, False, ep, dy2o, xmine, y_send.at[1], y_recv.at[1])
    dzb = Exchange(s, True, ep, dz2o, dz2i, z_send.at[1], z_recv.at[1])
    dz1o[...] = dot(pla[...], settled[:, :LANES]).astype(BF16).reshape(nz, zrows, LANES)
    dza.start()
    dy1o[...] = dot(plb[...], settled[:, LANES:]).astype(BF16).reshape(nyc, yrows, LANES)
    dyb.start()
    dza.wait_recv()
    moved = dot(pzy[...], dz1i[...].reshape(rows, LANES)).astype(BF16)
    dy2o[...] = moved.reshape(nyc, yrows, LANES)
    dya.start()
    dyb.wait_recv()
    moved = dot(pyz[...], dy1i[...].reshape(rows, LANES)).astype(BF16)
    dz2o[...] = moved.reshape(nz, zrows, LANES)
    dzb.start()

    def x_copy(i, src, dst, to):
        copy = pltpu.make_async_remote_copy(
            src_ref=src,
            dst_ref=dst,
            send_sem=x_send.at[i],
            recv_sem=x_recv.at[i],
            device_id={"tp": to},
            device_id_type=MESH,
        )
        sent.append(copy)
        return copy

    a_next = x_copy(0, xb.at[t, 0], xb.at[t, 0], nxt)
    b_next = x_copy(1, xb.at[t, 1], xb.at[t, 1], nxt)
    a_prev = x_copy(2, xb.at[t, 0], xb.at[t, 0], prv)
    b_prev = x_copy(3, xb.at[t, 1], xb.at[t, 1], prv)
    a_pass = x_copy(4, xb.at[prv, 0], xb.at[prv, 0], nxt)
    b_pass = x_copy(5, xb.at[nxt, 1], xb.at[nxt, 1], prv)
    dya.wait_recv()
    a_next.start()
    dzb.wait_recv()
    moved = dot(pzy[...], dz2i[...].reshape(rows, LANES)).astype(BF16)
    xb[t, 1] = moved.reshape(nyc, yrows, LANES)
    b_prev.start()
    b_next.start()
    a_prev.start()
    loads[6].wait()
    loads[7].wait()

    def hidden(i):
        x = jnp.concatenate([xb[i, 0].reshape(rows, LANES), xb[i, 1].reshape(rows, LANES)], axis=-1)
        at = pl.ds(pl.multiple_of(i * part, part), part)
        return dot(x, gate[at, :]), dot(x, up[at, :])

    g, u = hidden(t)
    gacc[...] = g
    uacc[...] = u
    a_next.wait_recv()
    a_pass.start()
    b_prev.wait_recv()
    b_pass.start()
    b_next.wait_recv()
    g, u = hidden(prv)
    gacc[...] += g
    uacc[...] += u
    a_prev.wait_recv()
    g, u = hidden(nxt)
    gacc[...] += g
    uacc[...] += u
    loads[8].wait()
    a_pass.wait_recv()
    b_pass.wait_recv()
    g, u = hidden(far)
    g = jnp.minimum(gacc[...] + g, LIMIT)
    u = jnp.clip(uacc[...] + u, -LIMIT, LIMIT)
    act = (g / (1.0 + jnp.exp(-SLOPE * g)) * (u + 1.0)).astype(BF16)

    def terms(i):
        return dot(act, down[:, pl.ds(pl.multiple_of(i * part, part), part)])

    a_far = x_copy(6, r2o.at[0], r2i.at[0], nxt)
    b_far = x_copy(7, r2o.at[1], r2i.at[1], prv)
    b_near = x_copy(8, rdo.at[0], rdi.at[0], nxt)
    a_near = x_copy(9, rdo.at[1], rdi.at[1], prv)
    a_pair = x_copy(10, rpo.at[0], rpi.at[0], nxt)
    b_pair = x_copy(11, rpo.at[1], rpi.at[1], prv)
    v = terms(far)
    r2o[0] = v[:, :LANES].astype(BF16)
    a_far.start()
    r2o[1] = v[:, LANES:].astype(BF16)
    b_far.start()
    vn = terms(nxt)
    rdo[0] = vn[:, LANES:].astype(BF16)
    b_near.start()
    vp = terms(prv)
    rdo[1] = vp[:, :LANES].astype(BF16)
    a_near.start()
    a_far.wait_recv()
    rpo[0] = (vn[:, :LANES] + r2i[0].astype(F32)).astype(BF16)
    a_pair.start()
    b_far.wait_recv()
    rpo[1] = (vp[:, LANES:] + r2i[1].astype(F32)).astype(BF16)
    b_pair.start()
    v = terms(t)
    eya = Exchange(s, False, ep, ey1o, ey1i, y_send.at[2], y_recv.at[2])
    ezb = Exchange(s, True, ep, ez1o, ez1i, z_send.at[2], z_recv.at[2])
    eza = Exchange(s, True, ep, ez2o, ez2i, z_send.at[3], z_recv.at[3])
    eyb = Exchange(s, False, ep, ey2o, ey2i, y_send.at[3], y_recv.at[3])
    a_near.wait_recv()
    a_pair.wait_recv()
    answer = v[:, :LANES] + rpi[0].astype(F32) + rdi[1].astype(F32)
    ey1o[...] = answer.astype(BF16).reshape(nyc, yrows, LANES)
    eya.start()
    b_near.wait_recv()
    b_pair.wait_recv()
    answer = v[:, LANES:] + rpi[1].astype(F32) + rdi[0].astype(F32)
    moved = dot(pyz[...], answer.astype(BF16)).astype(BF16)
    ez1o[...] = moved.reshape(nz, zrows, LANES)
    ezb.start()
    eya.wait_recv()
    moved = dot(pyz[...], ey1i[...].reshape(rows, LANES)).astype(BF16)
    ez2o[...] = moved.reshape(nz, zrows, LANES)
    eza.start()
    ezb.wait_recv()
    moved = dot(pzy[...], ez1i[...].reshape(rows, LANES)).astype(BF16)
    ey2o[...] = moved.reshape(nyc, yrows, LANES)
    eyb.start()

    def combined(c_ref, back):
        three = dot(c_ref[...], back[...].reshape(rows, LANES))
        return three[:group] + three[group : 2 * group] + three[2 * group :]

    eza.wait_recv()
    routed_a = combined(ca, ez2i)
    eyb.wait_recv()
    routed_b = combined(cb, ey2i)
    final = ALPHA * settled.astype(F32) + jnp.concatenate([routed_a, routed_b], axis=-1)
    out_ref[...] = normed(final, 4, stats2, gain2_ref)

    for copy in sent:
        copy.wait_send()
    for exchange in (dza, dyb, dya, dzb, eya, ezb, eza, eyb):
        exchange.wait_send()


def layer(
    nz,
    cap,
    tokens,
    lengths,
    key_cache,
    value_cache,
    query_weight,
    key_weight,
    value_weight,
    lambdas,
    head_gain,
    output_weight,
    norm1_gain,
    routes,
    route_logits,
    gate_weight,
    up_weight,
    down_weight,
    norm2_gain,
):
    tp = lax.axis_size("tp")
    own, width = tokens.shape
    blocks = width // LANES
    group = own * tp
    heads = lambdas.shape[0]
    length = key_cache.shape[1]
    s = Sizes(
        nz, lax.axis_size("ep") // nz, tp, own, blocks, heads, length, routes.shape[1], cap
    )
    half = key_weight.shape[1] // 4
    freqs = THETA ** (-jnp.arange(half, dtype=F32) / half)
    angles = lengths.astype(F32)[:, None] * freqs[None, :]
    cosine, sine = jnp.cos(angles), jnp.sin(angles)
    cosine = jnp.concatenate([cosine] * 4, axis=1)
    sine = jnp.concatenate([-sine, sine, -sine, sine], axis=1)
    rows, part = s.rows, width // tp
    tok = tokens.reshape(own, blocks, LANES).transpose(1, 0, 2).reshape(blocks * own, LANES)
    vmem = pl.BlockSpec(memory_space=pltpu.VMEM)
    smem = pl.BlockSpec(memory_space=pltpu.SMEM)
    hbm = pl.BlockSpec(memory_space=pl.ANY)

    def b(*shape):
        return pltpu.VMEM(shape, BF16)

    def f(*shape):
        return pltpu.VMEM(shape, F32)

    by_z = (nz, s.zrows, LANES)
    by_y = (s.nyc, s.yrows, LANES)
    sem = pltpu.SemaphoreType.DMA
    large = [query_weight, key_weight, value_weight, output_weight, key_cache, value_cache]
    large += [gate_weight[0], up_weight[0], down_weight[0]]
    landing = [large[i] for i in (0, 1, 2, 3, 4, 5, 6, 7, 8)]
    return pl.pallas_call(
        functools.partial(kernel, s),
        out_shape=jax.ShapeDtypeStruct((group, part), BF16),
        in_specs=[vmem, smem] + [vmem] * 5 + [smem] + [vmem] * 3 + [hbm] * 9,
        out_specs=vmem,
        scratch_shapes=[pltpu.VMEM(a.shape, a.dtype) for a in landing]
        + [
            b(tp, blocks * own, LANES),
            b(blocks, group, LANES),
            b(tp, group, LANES),
            f(group, LANES),
            f(group, LANES),
            b(tp, own * 2 * heads, LANES),
            f(tp, group, LANES),
            f(tp, group, LANES),
            b(rows, rows),
            b(rows, rows),
            b(rows, group),
            b(rows, group),
            b(3 * group, rows),
            b(3 * group, rows),
            b(*by_z),
            b(*by_z),
            b(*by_y),
            b(*by_y),
            b(*by_y),
            b(*by_z),
            b(*by_z),
            b(tp, 2, *by_y),
            f(rows, down_weight.shape[1]),
            f(rows, down_weight.shape[1]),
        ]
        + [b(2, rows, LANES)] * 6
        + [b(*by_y), b(*by_y), b(*by_z), b(*by_z)]
        + [b(*by_z), b(*by_z), b(*by_y), b(*by_y)]
        + [
            sem((9,)),
            sem((5, tp - 1)),
            sem((5, tp - 1)),
            sem((12,)),
            sem((12,)),
            sem((4, nz - 1)),
            sem((4, nz - 1)),
            sem((4, s.nyc - 1)),
            sem((4, s.nyc - 1)),
        ],
        compiler_params=pltpu.CompilerParams(collective_id=0, has_side_effects=True),
    )(
        tok,
        lengths,
        cosine,
        sine,
        routes,
        routes.T,
        route_logits,
        lambdas,
        head_gain.reshape(1, -1),
        norm1_gain.reshape(tp, part),
        norm2_gain.reshape(tp, part),
        *large,
    )


def solution(mesh, nz=8, cap=2):
    in_specs = (
        P(("ep", "tp"), None),
        P("ep"),
        P(("ep", "tp"), None, None),
        P(("ep", "tp"), None, None),
        P(None, "tp"),
        P(),
        P(),
        P(),
        P(),
        P(None, "tp"),
        P(),
        P("ep", None),
        P("ep", None),
        P("ep", None, "tp"),
        P("ep", None, "tp"),
        P("ep", "tp", None),
        P(),
    )
    return jax.shard_map(
        functools.partial(layer, nz, cap),
        mesh=mesh,
        in_specs=in_specs,
        out_specs=P("ep", "tp"),
        check_vma=False,
    )
```

time: 131 us -> 80.1 us (0.61)
  Pallas kernels: 0 us -> 74.3 us
  blocking collectives: 42.4 us -> 0 us
  waiting for transfers between devices: 37.7 us -> 0 us
  starting transfers between devices: 28.3 us -> 0 us
  local copies, waits for them, and re-layouts: 12.4 us -> 3.96 us
  matrix products: 4.71 us -> 0 us
  other arithmetic: 4.47 us -> 1.47 us
    pallas_call x0 -> x1, Pallas kernels: none -> 74.3 us  [layer(): pl.pallas_call(functools.partial(kernel, s), out_shape=jax.ShapeDtypeStru...]
    all_to_all x1 -> x0, blocking collectives: 42.4 us -> none  [body(): lax.all_to_all(outgoing, 'ep', split_axis=0, concat_axis=0, tiled=True)]
    all_to_all x7 -> x0, waiting for transfers between devices: 37.7 us -> none  [the longest x1 12.8 us: body(): lax.all_to_all(answers, 'ep', split_axis=0, concat_axis=0, tiled=True)]
    all_to_all x7 -> x0, starting transfers between devices: 28.3 us -> none  [the longest x4 14.7 us: copy_for_each(): lax.all_to_all(jnp.broadcast_to(x[None], (count, *x.shape)), axis, 0, 0,...]
    dot_general x11 -> x0, matrix products: 4.71 us -> none  [the longest x1 1.11 us: body(): jnp.dot(tokens, key_weight, preferred_element_type=f32)]
    broadcast_in_dim x4 -> x0, local copies, waits for them, and re-layouts: 3.28 us -> none  [copy_for_each(): jnp.broadcast_to(x[None], (count, *x.shape))]
    unnamed x28 -> x11, local copies, waits for them, and re-layouts: 5.31 us -> 2.77 us
    convert_element_type x5 -> x1, other arithmetic: 2.23 us -> 0.66 us  [layer(): angles = lengths.astype(F32)[:, None] * freqs[None, :]]
  transfers between devices with their start and end apart: 7 -> 0, of which waited for: 6 -> 0; matrix products, arithmetic and copies ran while one was open for 6% -> 0% of each run, Pallas kernels for 0% -> 0%
where the time goes in v1:
time: 80.1 us; the launch traced here: 79.8 us
  Pallas kernels  74.3 us (93%)
  local copies, waits for them, and re-layouts  3.96 us (5%)
  other arithmetic  1.47 us (2%)
    pallas_call x1, Pallas kernels, layer(): pl.pallas_call(functools.partial(kernel, s), out_shape=jax.ShapeDtypeStru...  74.3 us
    unnamed x11, local copies, waits for them, and re-layouts  2.77 us

profile of v1, /device:TPU:1, one launch (start us, length us, event | category | flops | bytes accessed | tf_op | source)
XLA Modules:
  0.0 79.8 jit_solution(6301928809891353369)
XLA Ops:
  0.0 0.7 convert_element_type.3
  0.7 0.1 fusion
  0.8 0.0 copy-start
  0.8 0.7 pad_maximum_fusion
  1.5 0.0 copy-done
  1.5 0.0 copy-start.1
  1.5 0.7 copy.19.routes_ref
  2.2 0.0 copy-done.1
  2.2 0.0 copy-start.2
  2.2 0.7 copy.20.logits_ref
  2.9 0.0 copy-done.2
  2.9 0.0 copy-start.3
  2.9 0.6 reshape.25.gain1_ref
  3.5 0.1 copy-done.3
  3.6 0.6 reshape.26.gain2_ref
  4.2 74.3 %shard_map.163 = bf16[16,256]{1,0:T(8,128)(2,1)} custom-call(bf16[32,128]{1,0:T(8,128)(2,1)} %bitcast.14, s32[16]{0:T(128)} %len_ref.1, f32[16,128]{1,0:T(8,128)} %get-tuple-element.8.cos_ref, f32[16,128]{1,0:T(8,128)} %get-tuple-element.9.sin_ref, s32[16,6]{1,0:T(8,128)} %copy.19.routes_ref, s32[6,16]{1,0:T(8,128)} %bitcast.13, f32[16,6]{1,0:T(8,128)} %copy.20.logits_ref, ...), custom_call_target="tpu_custom_call" | custom-call | tf_op jit(solution)/shard_map/pallas_call | solution.py:577
  78.5 1.3 %copy.22 = bf16[16,256]{1,0:T(8,128)(2,1)} copy(bf16[16,256]{1,0:T(8,128)(2,1)} %shard_map.163) | data formatting | bytes 16384
  (1 shorter events, 0.0 us)
Async XLA Ops:
  0.8 0.7 copy-start
  1.5 0.7 copy-start.1
  2.2 0.7 copy-start.2
  2.9 0.7 copy-start.3

commit v2 on v1

v2 whole, which is shorter than its diff:
```python
import functools

import jax
import jax.numpy as jnp
import numpy as np
from jax import lax
from jax.experimental import pallas as pl
from jax.experimental.pallas import tpu as pltpu
from jax.sharding import PartitionSpec as P

ALPHA = 1.4142135623730951
EPS = 1e-05
THETA = 500000.0
LIMIT = 7.0
SLOPE = 1.702
LANES = 128
SMALL = ("lens", "freqs", "routes", "logits", "lams", "hgain", "gain1", "gain2")
NAMES = SMALL + ("wq", "wk", "wv", "kc", "vc", "wo", "gate", "up", "down")
MESH = pl.DeviceIdType.MESH
BF16 = jnp.bfloat16
F32 = jnp.float32


def log2(n):
    return n.bit_length() - 1


def iota(shape, dim):
    return lax.broadcasted_iota(jnp.int32, shape, dim)


def ones_where(mask):
    return jnp.where(mask, 1.0, 0.0)


def dot(a, b):
    return jnp.dot(a, b, preferred_element_type=F32)


def zigzag(i, n):
    step = (i + 1) // 2
    return lax.rem(n // 2 + (1 - 2 * ((i + 1) % 2)) * step + n, n)


class Sizes:
    def __init__(self, nz, nyc, tp, own, blocks, heads, length, topk, cap):
        self.nz, self.nyc, self.tp, self.own = nz, nyc, tp, own
        self.blocks, self.heads, self.length = blocks, heads, length
        self.topk, self.cap = topk, cap
        self.group = own * tp
        self.experts = nz * nyc
        self.rows = nz * nyc * cap


class Exchange:
    def __init__(self, sizes, ep, out, into, send, recv):
        self.sizes, self.ep = sizes, ep
        self.out, self.into, self.send, self.recv = out, into, send, recv

    def peer(self, i):
        s = self.sizes
        z, y, c = self.ep // s.nyc, self.ep % s.nyc // 2, self.ep % 2
        j = i % s.nyc
        z = lax.rem(z + zigzag(i // s.nyc, s.nz), s.nz)
        y = lax.rem(y + zigzag(j // 2, s.nyc // 2), s.nyc // 2)
        return z * s.nyc + y * 2 + lax.rem(c + 1 - j % 2, 2)

    def start(self):
        def step(i, carry):
            other = self.peer(i)
            pltpu.make_async_remote_copy(
                src_ref=self.out.at[:, other],
                dst_ref=self.into.at[:, self.ep],
                send_sem=self.send,
                recv_sem=self.recv,
                device_id={"ep": other},
                device_id_type=MESH,
            ).start()
            return carry

        lax.fori_loop(0, self.sizes.experts - 1, step, 0)
        for half in range(2):
            self.into[half, self.ep] = self.out[half, self.ep]

    def total(self):
        every = pl.ds(0, self.sizes.experts - 1)
        return pltpu.make_async_remote_copy(
            src_ref=self.out.at[:, every],
            dst_ref=self.into.at[:, every],
            send_sem=self.send,
            recv_sem=self.recv,
            device_id={"ep": lax.rem(self.ep + 1, self.sizes.experts)},
            device_id_type=MESH,
        )

    def wait_recv(self):
        self.total().wait_recv()

    def wait_send(self):
        self.total().wait_send()


def rotation(angle):
    turns = jnp.floor(angle * 0.6366197723675814 + 0.5)
    r = angle - turns * 1.5703125
    r = r - turns * 4.837512969970703125e-4
    r = r - turns * 7.54978995489188216e-8
    q = r * r
    sine = r + r * q * (-1.6666654611e-1 + q * (8.3321608736e-3 - q * 1.9515295891e-4))
    cosine = 4.166664568298827e-2 + q * (-1.388731625493765e-3 + q * 2.443315711809948e-5)
    cosine = 1.0 - 0.5 * q + q * q * cosine
    quarter = turns.astype(jnp.int32)
    odd = (quarter & 1) == 1
    c = jnp.where(odd, sine, cosine)
    n = jnp.where(odd, cosine, sine)
    c = jnp.where(((quarter + 1) & 2) == 2, -c, c)
    n = jnp.where((quarter & 2) == 2, -n, n)
    return c, n


def kernel(
    s,
    *refs,
):
    count = len(NAMES)
    tok_hbm, inputs, out_ref = refs[0], refs[1 : count + 1], refs[count + 1]
    landing, refs = refs[count + 2 : 2 * count + 2], refs[2 * count + 2 :]
    (lens, freqs, routes_t, logits_t, lams, hgain, gain1, gain2) = landing[:8]
    (wq, wk, wv, kc, vc, wo, gate, up, down) = landing[8:]
    (tokbuf, xs, qbuf, nk_s, nv_s, len_s, attbuf, stats1, stats2, place, pick) = refs[:11]
    (dout, xb, gacc, uacc, r2o, r2i, rdo, rdi, rpo, rpi, eout, einto) = refs[11:23]
    (load_sem, tp_send, tp_recv, x_send, x_recv, ep_send, ep_recv, here) = refs[23:]
    ep = lax.axis_index("ep")
    t = lax.axis_index("tp")
    tp, own, group, heads = s.tp, s.own, s.group, s.heads
    rows, cap = s.rows, s.cap
    part = 2 * LANES
    nxt = lax.rem(t + 1, tp)
    far = lax.rem(t + 2, tp)
    prv = lax.rem(t + 3, tp)

    barrier = pltpu.get_barrier_semaphore()
    nz, ny = s.nz, s.nyc // 2
    z, y, c = ep // s.nyc, ep % s.nyc // 2, ep % 2

    def at_z(d):
        return {"ep": lax.rem(z + d + nz, nz) * s.nyc + ep % s.nyc}

    def at_y(d):
        return {"ep": z * s.nyc + lax.rem(y + d + ny, ny) * 2 + c}

    across = {"ep": ep + 1 - 2 * c}

    def pair(at, d, n):
        return [at(e) for e in sorted({d % n, -d % n} - {0})]

    near = pair(at_z, 1, nz) + pair(at_y, 1, ny) + [across]
    near += [{"tp": lax.rem(t + d, tp)} for d in range(1, tp)]
    for device in near:
        pl.semaphore_signal(barrier, inc=1, device_id=device, device_id_type=MESH)

    rounds = [
        pair(at_z, 1, nz),
        pair(at_z, 2, nz),
        pair(at_y, 1, ny),
        pair(at_y, 2, ny),
        pair(at_y, 4, ny),
        [across],
    ]

    def tell(i):
        for device in rounds[i]:
            pl.semaphore_signal(here.at[i], inc=1, device_id=device, device_id_type=MESH)

    def heard(i):
        if rounds[i]:
            pl.semaphore_wait(here.at[i], len(rounds[i]))

    tok_load = pltpu.make_async_copy(tok_hbm, tokbuf.at[t], load_sem.at[len(inputs)])
    tok_load.start()
    loads = {}
    for i, name in enumerate(NAMES):
        loads[name] = pltpu.make_async_copy(inputs[i], landing[i], load_sem.at[i])
        loads[name].start()

    for name in NAMES[:8]:
        loads[name].wait()
    lc = log2(cap)
    logits = logits_t[...]
    raised = jnp.exp(logits - jnp.max(logits, axis=0, keepdims=True))
    left = raised / jnp.sum(raised, axis=0, keepdims=True)
    named = routes_t[...].astype(F32)
    r0, c0 = iota((group, group), 0), iota((group, group), 1)
    upper = ones_where(r0 < c0).astype(BF16)
    lower = ones_where(c0 < r0).astype(BF16)
    same = ones_where(c0 == r0).astype(BF16)

    def upright(v):
        return lax.dot_general(
            same, v.astype(BF16), (((1,), (1,)), ((), ())), preferred_element_type=F32
        )

    routes = upright(named)
    pieces = []
    for i in range(3):
        pieces.append(left.astype(BF16))
        left = left - pieces[-1].astype(F32)
    route_weight = sum(upright(piece) for piece in pieces)
    row = iota((rows, group), 0)
    hits = jnp.zeros((rows, group), F32)
    for k in range(s.topk):
        hits += ones_where(named[k : k + 1, :] == (row >> lc).astype(F32))
    before = dot(hits.astype(BF16), upper)
    place[...] = jnp.where(before == (row & (cap - 1)).astype(F32), hits, 0.0).astype(BF16)
    row = iota((group, rows), 1)
    hits = jnp.zeros((group, rows), F32)
    weighed = jnp.zeros((group, rows), F32)
    for k in range(s.topk):
        hit = routes[:, k : k + 1] == (row >> lc).astype(F32)
        hits += ones_where(hit)
        weighed += jnp.where(hit, route_weight[:, k : k + 1], 0.0)
    before = dot(lower, hits.astype(BF16))
    weighed = jnp.where(before == (row & (cap - 1)).astype(F32), weighed, 0.0)
    for i in range(3):
        piece = weighed.astype(BF16)
        pick[i * group : (i + 1) * group, :] = piece
        weighed = weighed - piece.astype(F32)

    lane = iota((group, LANES), 1)
    lengths = jnp.where(c0 == r0, lens[...].astype(F32), 0.0)
    lengths = jnp.broadcast_to(jnp.sum(lengths, axis=-1, keepdims=True), (group, LANES))
    len_s[...] = lengths
    cosine, sine = rotation(lengths * freqs[...])
    sine = jnp.where((lane & 32) == 0, -sine, sine)
    r0, c0 = iota((2 * heads, heads), 0), iota((2 * heads, heads), 1)
    lam = jnp.where((r0 & (heads - 1)) == c0, lams[...], 0.0)
    lam = jnp.sum(lam, axis=-1, keepdims=True)

    def tp_copies(phase, src, buf):
        return [
            pltpu.make_async_remote_copy(
                src_ref=src,
                dst_ref=buf.at[t],
                send_sem=tp_send.at[phase, d - 1],
                recv_sem=tp_recv.at[phase, d - 1],
                device_id={"tp": lax.rem(t + d, tp)},
                device_id_type=MESH,
            )
            for d in (2, 1, 3)
        ]

    sent = []

    def gather(phase, src, buf):
        copies = tp_copies(phase, src, buf)
        for copy in copies:
            copy.start()
        sent.extend(copies)
        return copies

    def arrived(copies):
        for copy in copies:
            copy.wait_recv()

    tok_load.wait()
    pl.semaphore_wait(barrier, len(near))

    copies = gather(0, tokbuf.at[t], tokbuf)
    tell(0)
    nrow = tp * s.blocks * own
    r0, c0 = iota((nrow, nrow), 0), iota((nrow, nrow), 1)
    lo, lt, lb = log2(own), log2(tp), log2(s.blocks)
    origin = (((r0 >> lo) & (tp - 1)) << (lb + lo)) + ((r0 >> (lo + lt)) << lo) + (r0 & (own - 1))
    order = ones_where(c0 == origin).astype(BF16)
    loads["wq"].wait()
    arrived(copies)
    x = dot(order, tokbuf[...].reshape(nrow, LANES)).astype(BF16)
    xs[...] = x.reshape(s.blocks, group, LANES)
    x = jnp.concatenate([xs[i] for i in range(s.blocks)], axis=-1)

    def rotate(v):
        swapped = jnp.where((lane & 32) == 0, pltpu.roll(v, 96, 1), pltpu.roll(v, 32, 1))
        return (v * cosine + swapped * sine).astype(BF16)

    qbuf[t] = rotate(dot(x, wq[...]))
    copies = gather(1, qbuf.at[t], qbuf)
    heard(0)
    tell(1)
    loads["wk"].wait()
    loads["wv"].wait()
    nk_s[...] = rotate(dot(x, wk[...])).astype(F32)
    nv_s[...] = dot(x, wv[...]).astype(BF16).astype(F32)

    lh = log2(heads)
    nq = own * 2 * heads
    r0, c0 = iota((nq, heads * group), 0), iota((nq, heads * group), 1)
    source = ((r0 & (heads - 1)) * group) + t * own + (r0 >> (lh + 1))
    order = ones_where(c0 == source).astype(BF16)
    loads["kc"].wait()
    loads["vc"].wait()
    heard(1)
    tell(2)
    arrived(copies)
    q = dot(order, qbuf[...].reshape(heads * group, LANES))
    q = jnp.where((iota((nq, LANES), 1) >> 6) == ((iota((nq, LANES), 0) >> lh) & 1), q, 0.0)
    position = iota((2 * heads, s.length), 1).astype(F32)
    outs = []
    for b in range(own):
        qb = q[b * 2 * heads : (b + 1) * 2 * heads, :]
        score = lax.dot_general(
            qb.astype(BF16), kc[b], (((1,), (1,)), ((), ())), preferred_element_type=F32
        )
        length = jnp.concatenate([len_s[pl.ds(t * own + b, 1), :]] * (s.length // LANES), axis=-1)
        score = jnp.where(position < length, score * 0.125, -jnp.inf)
        own_score = jnp.sum(qb * nk_s[pl.ds(t * own + b, 1), :], axis=-1, keepdims=True) * 0.125
        top = jnp.maximum(jnp.max(score, axis=-1, keepdims=True), own_score)
        e = jnp.exp(score - top)
        e_own = jnp.exp(own_score - top)
        total = jnp.sum(e, axis=-1, keepdims=True) + e_own
        prob = e / total
        prob_own = jnp.broadcast_to(e_own / total, (2 * heads, LANES))
        weight = (prob - lam * pltpu.roll(prob, heads, 0)).astype(BF16)
        weight_own = (prob_own - lam * pltpu.roll(prob_own, heads, 0)).astype(BF16).astype(F32)
        ho = dot(weight, vc[b]) + weight_own * nv_s[pl.ds(t * own + b, 1), :]
        scale = lax.rsqrt(jnp.mean(ho * ho, axis=-1, keepdims=True) + EPS)
        outs.append(ho * scale * hgain[...])
    attbuf[t] = jnp.concatenate(outs, axis=0).astype(BF16)

    copies = gather(2, attbuf.at[t], attbuf)
    heard(2)
    tell(3)
    r0, c0 = iota((heads * group, tp * nq), 0), iota((heads * group, tp * nq), 1)
    lg = log2(group)
    token = r0 & (group - 1)
    source = (token >> lo) * nq + (token & (own - 1)) * (2 * heads) + (r0 >> lg)
    order = ones_where(c0 == source).astype(BF16)
    loads["wo"].wait()
    heard(3)
    tell(4)
    columns = jnp.concatenate([xs[2 * t], xs[2 * t + 1]], axis=-1).astype(F32)
    arrived(copies)
    att = dot(order, attbuf[...].reshape(tp * nq, LANES)).astype(BF16)
    att = jnp.concatenate([att[h * group : (h + 1) * group, :] for h in range(heads)], axis=-1)
    summed = ALPHA * columns + dot(att, wo[...])

    def normed(v, phase, stats, gain):
        mean = jnp.mean(v, axis=-1, keepdims=True)
        center = v - mean
        square = jnp.sum(center * center, axis=-1, keepdims=True)
        stats[t] = jnp.where(lane == 0, mean, jnp.where(lane == 1, square, 0.0))
        copies = gather(phase, stats.at[t], stats)
        if phase == 3:
            heard(4)
            tell(5)
        arrived(copies)
        means = [stats[i][:, 0:1] for i in range(tp)]
        squares = [stats[i][:, 1:2] for i in range(tp)]
        mean = sum(means) / tp
        spread = (sum(squares) + part * sum((m - mean) ** 2 for m in means)) / (tp * part)
        return ((v - mean) * lax.rsqrt(spread + EPS) * gain[:, pl.ds(pl.multiple_of(t * part, part), part)]).astype(BF16)

    settled = normed(summed, 3, stats1, gain1)

    by_expert = (s.experts, cap, LANES)
    there = Exchange(s, ep, dout, xb.at[t], ep_send.at[0], ep_recv.at[0])
    for half in range(2):
        v = dot(place[...], settled[:, half * LANES : (half + 1) * LANES]).astype(BF16)
        dout[half] = v.reshape(by_expert)
    heard(5)
    there.start()

    def x_copy(i, src, dst, to):
        copy = pltpu.make_async_remote_copy(
            src_ref=src,
            dst_ref=dst,
            send_sem=x_send.at[i],
            recv_sem=x_recv.at[i],
            device_id={"tp": to},
            device_id_type=MESH,
        )
        sent.append(copy)
        return copy

    a_next = x_copy(0, xb.at[t, 0], xb.at[t, 0], nxt)
    b_next = x_copy(1, xb.at[t, 1], xb.at[t, 1], nxt)
    a_prev = x_copy(2, xb.at[t, 0], xb.at[t, 0], prv)
    b_prev = x_copy(3, xb.at[t, 1], xb.at[t, 1], prv)
    a_pass = x_copy(4, xb.at[prv, 0], xb.at[prv, 0], nxt)
    b_pass = x_copy(5, xb.at[nxt, 1], xb.at[nxt, 1], prv)
    there.wait_recv()
    a_next.start()
    b_prev.start()
    b_next.start()
    a_prev.start()
    loads["gate"].wait()
    loads["up"].wait()

    def hidden(i):
        x = jnp.concatenate([xb[i, 0].reshape(rows, LANES), xb[i, 1].reshape(rows, LANES)], axis=-1)
        at = pl.ds(pl.multiple_of(i * part, part), part)
        return dot(x, gate[at, :]), dot(x, up[at, :])

    g, u = hidden(t)
    gacc[...] = g
    uacc[...] = u
    a_next.wait_recv()
    a_pass.start()
    b_prev.wait_recv()
    b_pass.start()
    b_next.wait_recv()
    g, u = hidden(prv)
    gacc[...] += g
    uacc[...] += u
    a_prev.wait_recv()
    g, u = hidden(nxt)
    gacc[...] += g
    uacc[...] += u
    loads["down"].wait()
    a_pass.wait_recv()
    b_pass.wait_recv()
    g, u = hidden(far)
    g = jnp.minimum(gacc[...] + g, LIMIT)
    u = jnp.clip(uacc[...] + u, -LIMIT, LIMIT)
    act = (g / (1.0 + jnp.exp(-SLOPE * g)) * (u + 1.0)).astype(BF16)

    def terms(i):
        return dot(act, down[:, pl.ds(pl.multiple_of(i * part, part), part)])

    a_far = x_copy(6, r2o.at[0], r2i.at[0], nxt)
    b_far = x_copy(7, r2o.at[1], r2i.at[1], prv)
    b_near = x_copy(8, rdo.at[0], rdi.at[0], nxt)
    a_near = x_copy(9, rdo.at[1], rdi.at[1], prv)
    a_pair = x_copy(10, rpo.at[0], rpi.at[0], nxt)
    b_pair = x_copy(11, rpo.at[1], rpi.at[1], prv)
    v = terms(far)
    r2o[0] = v[:, :LANES].astype(BF16)
    a_far.start()
    r2o[1] = v[:, LANES:].astype(BF16)
    b_far.start()
    vn = terms(nxt)
    rdo[0] = vn[:, LANES:].astype(BF16)
    b_near.start()
    vp = terms(prv)
    rdo[1] = vp[:, :LANES].astype(BF16)
    a_near.start()
    a_far.wait_recv()
    rpo[0] = (vn[:, :LANES] + r2i[0].astype(F32)).astype(BF16)
    a_pair.start()
    b_far.wait_recv()
    rpo[1] = (vp[:, LANES:] + r2i[1].astype(F32)).astype(BF16)
    b_pair.start()
    v = terms(t)
    back = Exchange(s, ep, eout, einto, ep_send.at[1], ep_recv.at[1])
    a_near.wait_recv()
    a_pair.wait_recv()
    answer = v[:, :LANES] + rpi[0].astype(F32) + rdi[1].astype(F32)
    eout[0] = answer.astype(BF16).reshape(by_expert)
    b_near.wait_recv()
    b_pair.wait_recv()
    answer = v[:, LANES:] + rpi[1].astype(F32) + rdi[0].astype(F32)
    eout[1] = answer.astype(BF16).reshape(by_expert)
    back.start()
    back.wait_recv()

    def combined(half):
        three = dot(pick[...], einto[half].reshape(rows, LANES))
        return three[:group] + three[group : 2 * group] + three[2 * group :]

    routed_a, routed_b = combined(0), combined(1)
    final = ALPHA * settled.astype(F32) + jnp.concatenate([routed_a, routed_b], axis=-1)
    out_ref[...] = normed(final, 4, stats2, gain2)

    for copy in sent:
        copy.wait_send()
    there.wait_send()
    back.wait_send()


def layer(
    nz,
    cap,
    tokens,
    lengths,
    key_cache,
    value_cache,
    query_weight,
    key_weight,
    value_weight,
    lambdas,
    head_gain,
    output_weight,
    norm1_gain,
    routes,
    route_logits,
    gate_weight,
    up_weight,
    down_weight,
    norm2_gain,
):
    tp = lax.axis_size("tp")
    own, width = tokens.shape
    blocks = width // LANES
    group = own * tp
    heads = lambdas.shape[0]
    length = key_cache.shape[1]
    s = Sizes(
        nz, lax.axis_size("ep") // nz, tp, own, blocks, heads, length, routes.shape[1], cap
    )
    rows, part = s.rows, width // tp
    half = key_weight.shape[1] // 4
    freqs = THETA ** (-np.arange(half, dtype=np.float32) / np.float32(half))
    freqs = np.concatenate([freqs] * 4).astype(np.float32).reshape(1, LANES)
    tok = tokens.reshape(own, blocks, LANES).transpose(1, 0, 2).reshape(blocks * own, LANES)
    given = dict(
        lens=lengths.reshape(1, -1),
        freqs=jnp.asarray(freqs),
        routes=routes.T,
        logits=route_logits.T,
        lams=lambdas.reshape(1, -1),
        hgain=head_gain.reshape(1, -1),
        gain1=norm1_gain.reshape(1, -1),
        gain2=norm2_gain.reshape(1, -1),
        wq=query_weight,
        wk=key_weight,
        wv=value_weight,
        kc=key_cache,
        vc=value_cache,
        wo=output_weight,
        gate=gate_weight[0],
        up=up_weight[0],
        down=down_weight[0],
    )
    operands = [given[name] for name in NAMES]

    def b(*shape):
        return pltpu.VMEM(shape, BF16)

    def f(*shape):
        return pltpu.VMEM(shape, F32)

    sem = pltpu.SemaphoreType.DMA
    by_expert = (s.experts, cap, LANES)
    ff = down_weight.shape[1]
    return pl.pallas_call(
        functools.partial(kernel, s),
        out_shape=jax.ShapeDtypeStruct((group, part), BF16),
        in_specs=[pl.BlockSpec(memory_space=pl.ANY)] * (1 + len(operands)),
        out_specs=pl.BlockSpec(memory_space=pltpu.VMEM),
        scratch_shapes=[pltpu.VMEM(a.shape, a.dtype) for a in operands]
        + [
            b(tp, blocks * own, LANES),
            b(blocks, group, LANES),
            b(tp, group, LANES),
            f(group, LANES),
            f(group, LANES),
            f(group, LANES),
            b(tp, own * 2 * heads, LANES),
            f(tp, group, LANES),
            f(tp, group, LANES),
            b(rows, group),
            b(3 * group, rows),
            b(2, *by_expert),
            b(tp, 2, *by_expert),
            f(rows, ff),
            f(rows, ff),
        ]
        + [b(2, rows, LANES)] * 6
        + [b(2, *by_expert)] * 2
        + [
            sem((1 + len(operands),)),
            sem((5, tp - 1)),
            sem((5, tp - 1)),
            sem((12,)),
            sem((12,)),
            sem((2,)),
            sem((2,)),
            pltpu.SemaphoreType.REGULAR((6,)),
        ],
        compiler_params=pltpu.CompilerParams(collective_id=0, has_side_effects=True),
    )(tok, *operands)


def solution(mesh, nz=8, cap=2):
    in_specs = (
        P(("ep", "tp"), None),
        P("ep"),
        P(("ep", "tp"), None, None),
        P(("ep", "tp"), None, None),
        P(None, "tp"),
        P(),
        P(),
        P(),
        P(),
        P(None, "tp"),
        P(),
        P("ep", None),
        P("ep", None),
        P("ep", None, "tp"),
        P("ep", None, "tp"),
        P("ep", "tp", None),
        P(),
    )
    return jax.shard_map(
        functools.partial(layer, nz, cap),
        mesh=mesh,
        in_specs=in_specs,
        out_specs=P("ep", "tp"),
        check_vma=False,
    )
```

time: 80.1 us -> 72.8 us (0.909)
  Pallas kernels: 74.3 us -> 71.3 us
  local copies, waits for them, and re-layouts: 3.96 us -> 1.3 us
  other arithmetic: 1.47 us -> 0 us
    pallas_call x1, Pallas kernels: 74.3 us -> 71.3 us  [layer(): pl.pallas_call(functools.partial(kernel, s), out_shape=jax.ShapeDtypeStru...]
    unnamed x11 -> x1, local copies, waits for them, and re-layouts: 2.77 us -> 1.3 us
    reshape x2 -> x0, local copies, waits for them, and re-layouts: 1.19 us -> none  [the longest x1 0.6 us: layer(): norm2_gain.reshape(tp, part)]
where the time goes in v2:
time: 72.8 us; the launch traced here: 72.7 us
  Pallas kernels  71.3 us (98%)
  local copies, waits for them, and re-layouts  1.3 us (2%)
    pallas_call x1, Pallas kernels, layer(): pl.pallas_call(functools.partial(kernel, s), out_shape=jax.ShapeDtypeStru...  71.3 us

profile of v2, /device:TPU:1, one launch (start us, length us, event | category | flops | bytes accessed | tf_op | source)
XLA Modules:
  0.0 72.7 jit_solution(14788553181299873145)
XLA Ops:
  0.0 71.3 %shard_map.172 = bf16[16,256]{1,0:T(8,128)(2,1)} custom-call(bf16[32,128]{1,0:T(8,128)(2,1)} %bitcast.18, s32[1,16]{1,0:T(1,128)} %bitcast.23, f32[1,128]{1,0:T(1,128)} %constant.2.clone.refs_2_, s32[6,16]{1,0:T(8,128)} %bitcast.19, f32[6,16]{1,0:T(8,128)} %bitcast.20, f32[1,4]{1,0:T(1,128)} %bitcast.24, f32[1,128]{1,0:T(1,128)} %bitcast.25, ...), custom_call_target="tpu_custom_call" | custom-call | tf_op jit(solution)/shard_map/pallas_call | solution.py:544
  71.4 1.3 %copy.21 = bf16[16,256]{1,0:T(8,128)(2,1)} copy(bf16[16,256]{1,0:T(8,128)(2,1)} %shard_map.172) | data formatting | bytes 16384

commit v3 on v2

--- a/solution.py
+++ b/solution.py
@@ -37,9 +37,8 @@
     return jnp.dot(a, b, preferred_element_type=F32)
 
 
-def zigzag(i, n):
-    step = (i + 1) // 2
-    return lax.rem(n // 2 + (1 - 2 * ((i + 1) % 2)) * step + n, n)
+def far_first(n):
+    return sorted(range(n), key=lambda d: -min(d, n - d))
 
 
 class Sizes:
@@ -57,17 +56,10 @@
         self.sizes, self.ep = sizes, ep
         self.out, self.into, self.send, self.recv = out, into, send, recv
 
-    def peer(self, i):
-        s = self.sizes
-        z, y, c = self.ep // s.nyc, self.ep % s.nyc // 2, self.ep % 2
-        j = i % s.nyc
-        z = lax.rem(z + zigzag(i // s.nyc, s.nz), s.nz)
-        y = lax.rem(y + zigzag(j // 2, s.nyc // 2), s.nyc // 2)
-        return z * s.nyc + y * 2 + lax.rem(c + 1 - j % 2, 2)
-
-    def start(self):
-        def step(i, carry):
-            other = self.peer(i)
+    def start(self, lines):
+        planes, tails = lines
+
+        def post(other):
             pltpu.make_async_remote_copy(
                 src_ref=self.out.at[:, other],
                 dst_ref=self.into.at[:, self.ep],
@@ -76,9 +68,11 @@
                 device_id={"ep": other},
                 device_id_type=MESH,
             ).start()
-            return carry
-
-        lax.fori_loop(0, self.sizes.experts - 1, step, 0)
+
+        for plane in planes:
+            for tail in tails:
+                if plane is not planes[-1] or tail is not tails[-1]:
+                    post(plane + tail)
         for half in range(2):
             self.into[half, self.ep] = self.out[half, self.ep]
 
@@ -183,6 +177,40 @@
         loads[name] = pltpu.make_async_copy(inputs[i], landing[i], load_sem.at[i])
         loads[name].start()
 
+    def tp_copies(phase, src, buf):
+        return [
+            pltpu.make_async_remote_copy(
+                src_ref=src,
+                dst_ref=buf.at[t],
+                send_sem=tp_send.at[phase, d - 1],
+                recv_sem=tp_recv.at[phase, d - 1],
+                device_id={"tp": lax.rem(t + d, tp)},
+                device_id_type=MESH,
+            )
+            for d in (2, 1, 3)
+        ]
+
+    sent = []
+
+    def gather(phase, src, buf):
+        copies = tp_copies(phase, src, buf)
+        for copy in copies:
+            copy.start()
+        sent.extend(copies)
+        return copies
+
+    def arrived(copies):
+        for copy in copies:
+            copy.wait_recv()
+
+    tok_load.wait()
+    pl.semaphore_wait(barrier, len(near))
+
+    copies = gather(0, tokbuf.at[t], tokbuf)
+    tell(0)
+    planes = [lax.rem(z + d, nz) * s.nyc for d in far_first(nz)]
+    columns = [lax.rem(y + d, ny) * 2 for d in far_first(ny)]
+    lines = planes, [column + core for column in columns for core in (1 - c, c)]
     for name in NAMES[:8]:
         loads[name].wait()
     lc = log2(cap)
@@ -236,37 +264,6 @@
     lam = jnp.where((r0 & (heads - 1)) == c0, lams[...], 0.0)
     lam = jnp.sum(lam, axis=-1, keepdims=True)
 
-    def tp_copies(phase, src, buf):
-        return [
-            pltpu.make_async_remote_copy(
-                src_ref=src,
-                dst_ref=buf.at[t],
-                send_sem=tp_send.at[phase, d - 1],
-                recv_sem=tp_recv.at[phase, d - 1],
-                device_id={"tp": lax.rem(t + d, tp)},
-                device_id_type=MESH,
-            )
-            for d in (2, 1, 3)
-        ]
-
-    sent = []
-
-    def gather(phase, src, buf):
-        copies = tp_copies(phase, src, buf)
-        for copy in copies:
-            copy.start()
-        sent.extend(copies)
-        return copies
-
-    def arrived(copies):
-        for copy in copies:
-            copy.wait_recv()
-
-    tok_load.wait()
-    pl.semaphore_wait(barrier, len(near))
-
-    copies = gather(0, tokbuf.at[t], tokbuf)
-    tell(0)
     nrow = tp * s.blocks * own
     r0, c0 = iota((nrow, nrow), 0), iota((nrow, nrow), 1)
     lo, lt, lb = log2(own), log2(tp), log2(s.blocks)
@@ -367,7 +364,7 @@
         v = dot(place[...], settled[:, half * LANES : (half + 1) * LANES]).astype(BF16)
         dout[half] = v.reshape(by_expert)
     heard(5)
-    there.start()
+    there.start(lines)
 
     def x_copy(i, src, dst, to):
         copy = pltpu.make_async_remote_copy(
@@ -459,7 +456,7 @@
     b_pair.wait_recv()
     answer = v[:, LANES:] + rpi[1].astype(F32) + rdi[0].astype(F32)
     eout[1] = answer.astype(BF16).reshape(by_expert)
-    back.start()
+    back.start(lines)
     back.wait_recv()
 
     def combined(half):
@@ -576,7 +573,9 @@
             sem((2,)),
             pltpu.SemaphoreType.REGULAR((6,)),
         ],
-        compiler_params=pltpu.CompilerParams(collective_id=0, has_side_effects=True),
+        compiler_params=pltpu.CompilerParams(
+            collective_id=0, has_side_effects=True
+        ),
     )(tok, *operands)
 
 

time: 72.8 us -> 65.9 us (0.905)
  Pallas kernels: 71.3 us -> 64.4 us
    pallas_call x1, Pallas kernels: 71.3 us -> 64.4 us  [layer(): pl.pallas_call(functools.partial(kernel, s), out_shape=jax.ShapeDtypeStru...]
where the time goes in v3:
time: 65.9 us; the launch traced here: 65.7 us
  Pallas kernels  64.4 us (98%)
  local copies, waits for them, and re-layouts  1.3 us (2%)
    pallas_call x1, Pallas kernels, layer(): pl.pallas_call(functools.partial(kernel, s), out_shape=jax.ShapeDtypeStru...  64.4 us

profile of v3, /device:TPU:1, one launch (start us, length us, event | category | flops | bytes accessed | tf_op | source)
XLA Modules:
  0.0 65.7 jit_solution(5815882324435969155)
XLA Ops:
  0.0 64.4 %shard_map.172 = bf16[16,256]{1,0:T(8,128)(2,1)} custom-call(bf16[32,128]{1,0:T(8,128)(2,1)} %bitcast.18, s32[1,16]{1,0:T(1,128)} %bitcast.23, f32[1,128]{1,0:T(1,128)} %constant.2.clone.refs_2_, s32[6,16]{1,0:T(8,128)} %bitcast.19, f32[6,16]{1,0:T(8,128)} %bitcast.20, f32[1,4]{1,0:T(1,128)} %bitcast.24, f32[1,128]{1,0:T(1,128)} %bitcast.25, ...), custom_call_target="tpu_custom_call" | custom-call | tf_op jit(solution)/shard_map/pallas_call | solution.py:541
  64.4 1.3 %copy.21 = bf16[16,256]{1,0:T(8,128)(2,1)} copy(bf16[16,256]{1,0:T(8,128)(2,1)} %shard_map.172) | data formatting | bytes 16384

commit v4 on v3

--- a/solution.py
+++ b/solution.py
@@ -51,47 +51,27 @@
         self.rows = nz * nyc * cap
 
 
-class Exchange:
-    def __init__(self, sizes, ep, out, into, send, recv):
-        self.sizes, self.ep = sizes, ep
-        self.out, self.into, self.send, self.recv = out, into, send, recv
-
-    def start(self, lines):
-        planes, tails = lines
-
-        def post(other):
-            pltpu.make_async_remote_copy(
-                src_ref=self.out.at[:, other],
-                dst_ref=self.into.at[:, self.ep],
-                send_sem=self.send,
-                recv_sem=self.recv,
-                device_id={"ep": other},
-                device_id_type=MESH,
-            ).start()
-
-        for plane in planes:
-            for tail in tails:
-                if plane is not planes[-1] or tail is not tails[-1]:
-                    post(plane + tail)
-        for half in range(2):
-            self.into[half, self.ep] = self.out[half, self.ep]
-
-    def total(self):
-        every = pl.ds(0, self.sizes.experts - 1)
-        return pltpu.make_async_remote_copy(
-            src_ref=self.out.at[:, every],
-            dst_ref=self.into.at[:, every],
-            send_sem=self.send,
-            recv_sem=self.recv,
-            device_id={"ep": lax.rem(self.ep + 1, self.sizes.experts)},
-            device_id_type=MESH,
-        )
-
-    def wait_recv(self):
-        self.total().wait_recv()
-
-    def wait_send(self):
-        self.total().wait_send()
+def post(src, dst, send, recv, device):
+    pltpu.make_async_remote_copy(
+        src_ref=src,
+        dst_ref=dst,
+        send_sem=send,
+        recv_sem=recv,
+        device_id={"ep": device},
+        device_id_type=MESH,
+    ).start()
+
+
+def messages(ref, count, send, recv, device):
+    some = ref.at[:, pl.ds(0, count)]
+    return pltpu.make_async_remote_copy(
+        src_ref=some,
+        dst_ref=some,
+        send_sem=send,
+        recv_sem=recv,
+        device_id={"ep": device},
+        device_id_type=MESH,
+    )
 
 
 def rotation(angle):
@@ -122,8 +102,8 @@
     (lens, freqs, routes_t, logits_t, lams, hgain, gain1, gain2) = landing[:8]
     (wq, wk, wv, kc, vc, wo, gate, up, down) = landing[8:]
     (tokbuf, xs, qbuf, nk_s, nv_s, len_s, attbuf, stats1, stats2, place, pick) = refs[:11]
-    (dout, xb, gacc, uacc, r2o, r2i, rdo, rdi, rpo, rpi, eout, einto) = refs[11:23]
-    (load_sem, tp_send, tp_recv, x_send, x_recv, ep_send, ep_recv, here) = refs[23:]
+    (dout, xb, r2o, r2i, rdo, rdi, rpo, rpi, eout, einto) = refs[11:21]
+    (load_sem, tp_send, tp_recv, x_send, x_recv, ep_send, ep_recv, here) = refs[21:]
     ep = lax.axis_index("ep")
     t = lax.axis_index("tp")
     tp, own, group, heads = s.tp, s.own, s.group, s.heads
@@ -175,7 +155,6 @@
     loads = {}
     for i, name in enumerate(NAMES):
         loads[name] = pltpu.make_async_copy(inputs[i], landing[i], load_sem.at[i])
-        loads[name].start()
 
     def tp_copies(phase, src, buf):
         return [
@@ -208,9 +187,13 @@
 
     copies = gather(0, tokbuf.at[t], tokbuf)
     tell(0)
+    for load in loads.values():
+        load.start()
     planes = [lax.rem(z + d, nz) * s.nyc for d in far_first(nz)]
+    origins = [lax.rem(z - d + nz, nz) * s.nyc for d in far_first(nz)]
     columns = [lax.rem(y + d, ny) * 2 for d in far_first(ny)]
-    lines = planes, [column + core for column in columns for core in (1 - c, c)]
+    tails = [column + core for column in columns for core in (1 - c, c)]
+    line = ep % s.nyc
     for name in NAMES[:8]:
         loads[name].wait()
     lc = log2(cap)
@@ -314,8 +297,9 @@
         e = jnp.exp(score - top)
         e_own = jnp.exp(own_score - top)
         total = jnp.sum(e, axis=-1, keepdims=True) + e_own
-        prob = e / total
-        prob_own = jnp.broadcast_to(e_own / total, (2 * heads, LANES))
+        share = 1.0 / total
+        prob = e * share
+        prob_own = jnp.broadcast_to(e_own * share, (2 * heads, LANES))
         weight = (prob - lam * pltpu.roll(prob, heads, 0)).astype(BF16)
         weight_own = (prob_own - lam * pltpu.roll(prob_own, heads, 0)).astype(BF16).astype(F32)
         ho = dot(weight, vc[b]) + weight_own * nv_s[pl.ds(t * own + b, 1), :]
@@ -359,12 +343,19 @@
     settled = normed(summed, 3, stats1, gain1)
 
     by_expert = (s.experts, cap, LANES)
-    there = Exchange(s, ep, dout, xb.at[t], ep_send.at[0], ep_recv.at[0])
+    mid, last = nz // 2, s.nyc - 1
     for half in range(2):
         v = dot(place[...], settled[:, half * LANES : (half + 1) * LANES]).astype(BF16)
         dout[half] = v.reshape(by_expert)
     heard(5)
-    there.start(lines)
+    for i in range(nz):
+        for j in range(s.nyc):
+            if i < nz - 1 or j < last:
+                other = planes[i] + tails[j]
+                slot = i * s.nyc + line
+                post(dout.at[:, other], xb.at[t, :, slot], ep_send.at[0], ep_recv.at[i // mid], other)
+    for half in range(2):
+        xb[t, half, (nz - 1) * s.nyc + line] = dout[half, ep]
 
     def x_copy(i, src, dst, to):
         copy = pltpu.make_async_remote_copy(
@@ -378,86 +369,110 @@
         sent.append(copy)
         return copy
 
-    a_next = x_copy(0, xb.at[t, 0], xb.at[t, 0], nxt)
-    b_next = x_copy(1, xb.at[t, 1], xb.at[t, 1], nxt)
-    a_prev = x_copy(2, xb.at[t, 0], xb.at[t, 0], prv)
-    b_prev = x_copy(3, xb.at[t, 1], xb.at[t, 1], prv)
-    a_pass = x_copy(4, xb.at[prv, 0], xb.at[prv, 0], nxt)
-    b_pass = x_copy(5, xb.at[nxt, 1], xb.at[nxt, 1], prv)
-    there.wait_recv()
-    a_next.start()
-    b_prev.start()
-    b_next.start()
-    a_prev.start()
+    slots = s.experts // 2
+    some = rows // 2
+    neighbour = across["ep"]
+    a_next, b_next, a_prev, b_prev, a_pass, b_pass = [], [], [], [], [], []
+    for p in range(2):
+        at = pl.ds(p * slots, slots)
+
+        def round_x(i, who, half, to, p=p, at=at):
+            return x_copy(12 * p + i, xb.at[who, half, at], xb.at[who, half, at], to)
+
+        a_next.append(round_x(0, t, 0, nxt))
+        b_next.append(round_x(1, t, 1, nxt))
+        a_prev.append(round_x(2, t, 0, prv))
+        b_prev.append(round_x(3, t, 1, prv))
+        a_pass.append(round_x(4, prv, 0, nxt))
+        b_pass.append(round_x(5, nxt, 1, prv))
+
+    for p in range(2):
+        messages(dout, slots - p, ep_send.at[0], ep_recv.at[p], neighbour).wait_recv()
+        a_next[p].start()
+        b_prev[p].start()
+        b_next[p].start()
+        a_prev[p].start()
+    for p in range(2):
+        a_next[p].wait_recv()
+        a_pass[p].start()
+        b_prev[p].wait_recv()
+        b_pass[p].start()
     loads["gate"].wait()
     loads["up"].wait()
-
-    def hidden(i):
-        x = jnp.concatenate([xb[i, 0].reshape(rows, LANES), xb[i, 1].reshape(rows, LANES)], axis=-1)
-        at = pl.ds(pl.multiple_of(i * part, part), part)
-        return dot(x, gate[at, :]), dot(x, up[at, :])
-
-    g, u = hidden(t)
-    gacc[...] = g
-    uacc[...] = u
-    a_next.wait_recv()
-    a_pass.start()
-    b_prev.wait_recv()
-    b_pass.start()
-    b_next.wait_recv()
-    g, u = hidden(prv)
-    gacc[...] += g
-    uacc[...] += u
-    a_prev.wait_recv()
-    g, u = hidden(nxt)
-    gacc[...] += g
-    uacc[...] += u
     loads["down"].wait()
-    a_pass.wait_recv()
-    b_pass.wait_recv()
-    g, u = hidden(far)
-    g = jnp.minimum(gacc[...] + g, LIMIT)
-    u = jnp.clip(uacc[...] + u, -LIMIT, LIMIT)
-    act = (g / (1.0 + jnp.exp(-SLOPE * g)) * (u + 1.0)).astype(BF16)
-
-    def terms(i):
+
+    def hidden(p):
+        at = pl.ds(p * slots, slots)
+        g = u = 0.0
+        for i in (t, prv, nxt, far):
+            x = [xb[i, half, at].reshape(some, LANES) for half in range(2)]
+            x = jnp.concatenate(x, axis=-1)
+            k = pl.ds(pl.multiple_of(i * part, part), part)
+            g = g + dot(x, gate[k, :])
+            u = u + dot(x, up[k, :])
+        g = jnp.minimum(g, LIMIT)
+        u = jnp.clip(u, -LIMIT, LIMIT)
+        return (g / (1.0 + jnp.exp(-SLOPE * g)) * (u + 1.0)).astype(BF16)
+
+    def terms(act, i):
         return dot(act, down[:, pl.ds(pl.multiple_of(i * part, part), part)])
 
-    a_far = x_copy(6, r2o.at[0], r2i.at[0], nxt)
-    b_far = x_copy(7, r2o.at[1], r2i.at[1], prv)
-    b_near = x_copy(8, rdo.at[0], rdi.at[0], nxt)
-    a_near = x_copy(9, rdo.at[1], rdi.at[1], prv)
-    a_pair = x_copy(10, rpo.at[0], rpi.at[0], nxt)
-    b_pair = x_copy(11, rpo.at[1], rpi.at[1], prv)
-    v = terms(far)
-    r2o[0] = v[:, :LANES].astype(BF16)
-    a_far.start()
-    r2o[1] = v[:, LANES:].astype(BF16)
-    b_far.start()
-    vn = terms(nxt)
-    rdo[0] = vn[:, LANES:].astype(BF16)
-    b_near.start()
-    vp = terms(prv)
-    rdo[1] = vp[:, :LANES].astype(BF16)
-    a_near.start()
-    a_far.wait_recv()
-    rpo[0] = (vn[:, :LANES] + r2i[0].astype(F32)).astype(BF16)
-    a_pair.start()
-    b_far.wait_recv()
-    rpo[1] = (vp[:, LANES:] + r2i[1].astype(F32)).astype(BF16)
-    b_pair.start()
-    v = terms(t)
-    back = Exchange(s, ep, eout, einto, ep_send.at[1], ep_recv.at[1])
-    a_near.wait_recv()
-    a_pair.wait_recv()
-    answer = v[:, :LANES] + rpi[0].astype(F32) + rdi[1].astype(F32)
-    eout[0] = answer.astype(BF16).reshape(by_expert)
-    b_near.wait_recv()
-    b_pair.wait_recv()
-    answer = v[:, LANES:] + rpi[1].astype(F32) + rdi[0].astype(F32)
-    eout[1] = answer.astype(BF16).reshape(by_expert)
-    back.start(lines)
-    back.wait_recv()
+    acts, pairs, sums = [], [], []
+    for p in range(2):
+        b_next[p].wait_recv()
+        a_prev[p].wait_recv()
+        a_pass[p].wait_recv()
+        b_pass[p].wait_recv()
+        act = hidden(p)
+        acts.append(act)
+        hops = [
+            x_copy(12 * p + 6, r2o.at[p, 0], r2i.at[p, 0], nxt),
+            x_copy(12 * p + 7, r2o.at[p, 1], r2i.at[p, 1], prv),
+            x_copy(12 * p + 8, rdo.at[p, 0], rdi.at[p, 0], nxt),
+            x_copy(12 * p + 9, rdo.at[p, 1], rdi.at[p, 1], prv),
+            x_copy(12 * p + 10, rpo.at[p, 0], rpi.at[p, 0], nxt),
+            x_copy(12 * p + 11, rpo.at[p, 1], rpi.at[p, 1], prv),
+        ]
+        sums.append(hops)
+        v = terms(act, far)
+        r2o[p, 0] = v[:, :LANES].astype(BF16)
+        hops[0].start()
+        r2o[p, 1] = v[:, LANES:].astype(BF16)
+        hops[1].start()
+        vn = terms(act, nxt)
+        rdo[p, 0] = vn[:, LANES:].astype(BF16)
+        hops[2].start()
+        vp = terms(act, prv)
+        rdo[p, 1] = vp[:, :LANES].astype(BF16)
+        hops[3].start()
+        pairs.append((vn[:, :LANES], vp[:, LANES:]))
+    for p in range(2):
+        hops, (vn, vp) = sums[p], pairs[p]
+        hops[0].wait_recv()
+        rpo[p, 0] = (vn + r2i[p, 0].astype(F32)).astype(BF16)
+        hops[4].start()
+        hops[1].wait_recv()
+        rpo[p, 1] = (vp + r2i[p, 1].astype(F32)).astype(BF16)
+        hops[5].start()
+    mine = [terms(act, t) for act in acts]
+    for p in range(2):
+        hops, v = sums[p], mine[p]
+        at = pl.ds(p * slots, slots)
+        for i in (2, 3, 4, 5):
+            hops[i].wait_recv()
+        answer = v[:, :LANES] + rpi[p, 0].astype(F32) + rdi[p, 1].astype(F32)
+        eout[0, at] = answer.astype(BF16).reshape(slots, cap, LANES)
+        answer = v[:, LANES:] + rpi[p, 1].astype(F32) + rdi[p, 0].astype(F32)
+        eout[1, at] = answer.astype(BF16).reshape(slots, cap, LANES)
+        for i in range(p * mid, (p + 1) * mid):
+            for j in range(s.nyc):
+                if i < nz - 1 or j < last:
+                    slot = i * s.nyc + tails[j]
+                    other = origins[i] + tails[j]
+                    post(eout.at[:, slot], einto.at[:, ep], ep_send.at[1], ep_recv.at[2], other)
+    for half in range(2):
+        einto[half, ep] = eout[half, (nz - 1) * s.nyc + line]
+    messages(eout, s.experts - 1, ep_send.at[1], ep_recv.at[2], neighbour).wait_recv()
 
     def combined(half):
         three = dot(pick[...], einto[half].reshape(rows, LANES))
@@ -469,8 +484,8 @@
 
     for copy in sent:
         copy.wait_send()
-    there.wait_send()
-    back.wait_send()
+    messages(dout, s.experts - 1, ep_send.at[0], ep_recv.at[0], neighbour).wait_send()
+    messages(eout, s.experts - 1, ep_send.at[1], ep_recv.at[2], neighbour).wait_send()
 
 
 def layer(
@@ -537,7 +552,6 @@
 
     sem = pltpu.SemaphoreType.DMA
     by_expert = (s.experts, cap, LANES)
-    ff = down_weight.shape[1]
     return pl.pallas_call(
         functools.partial(kernel, s),
         out_shape=jax.ShapeDtypeStruct((group, part), BF16),
@@ -558,19 +572,17 @@
             b(3 * group, rows),
             b(2, *by_expert),
             b(tp, 2, *by_expert),
-            f(rows, ff),
-            f(rows, ff),
         ]
-        + [b(2, rows, LANES)] * 6
+        + [b(2, 2, rows // 2, LANES)] * 6
         + [b(2, *by_expert)] * 2
         + [
             sem((1 + len(operands),)),
             sem((5, tp - 1)),
             sem((5, tp - 1)),
-            sem((12,)),
-            sem((12,)),
+            sem((24,)),
+            sem((24,)),
             sem((2,)),
-            sem((2,)),
+            sem((3,)),
             pltpu.SemaphoreType.REGULAR((6,)),
         ],
         compiler_params=pltpu.CompilerParams(

time: 65.9 us -> 64.7 us (0.982)
  Pallas kernels: 64.4 us -> 63.1 us
    pallas_call x1, Pallas kernels: 64.4 us -> 63.1 us  [layer(): pl.pallas_call(functools.partial(kernel, s), out_shape=jax.ShapeDtypeStru...]
where the time goes in v4:
time: 64.7 us; the launch traced here: 64.4 us
  Pallas kernels  63.1 us (98%)
  local copies, waits for them, and re-layouts  1.3 us (2%)
    pallas_call x1, Pallas kernels, layer(): pl.pallas_call(functools.partial(kernel, s), out_shape=jax.ShapeDtypeStru...  63.1 us
    unnamed x1, local copies, waits for them, and re-layouts  1.3 us

profile of v4, /device:TPU:1, one launch (start us, length us, event | category | flops | bytes accessed | tf_op | source)
XLA Modules:
  0.0 64.4 jit_solution(2478906893736847144)
XLA Ops:
  0.0 63.1 %shard_map.172 = bf16[16,256]{1,0:T(8,128)(2,1)} custom-call(bf16[32,128]{1,0:T(8,128)(2,1)} %bitcast.18, s32[1,16]{1,0:T(1,128)} %bitcast.23, f32[1,128]{1,0:T(1,128)} %constant.2.clone.refs_2_, s32[6,16]{1,0:T(8,128)} %bitcast.19, f32[6,16]{1,0:T(8,128)} %bitcast.20, f32[1,4]{1,0:T(1,128)} %bitcast.24, f32[1,128]{1,0:T(1,128)} %bitcast.25, ...), custom_call_target="tpu_custom_call" | custom-call | tf_op jit(solution)/shard_map/pallas_call | solution.py:555
  63.1 1.3 %copy.21 = bf16[16,256]{1,0:T(8,128)(2,1)} copy(bf16[16,256]{1,0:T(8,128)(2,1)} %shard_map.172) | data formatting | bytes 16384

commit v5 on v4

--- a/solution.py
+++ b/solution.py
@@ -102,8 +102,8 @@
     (lens, freqs, routes_t, logits_t, lams, hgain, gain1, gain2) = landing[:8]
     (wq, wk, wv, kc, vc, wo, gate, up, down) = landing[8:]
     (tokbuf, xs, qbuf, nk_s, nv_s, len_s, attbuf, stats1, stats2, place, pick) = refs[:11]
-    (dout, xb, r2o, r2i, rdo, rdi, rpo, rpi, eout, einto) = refs[11:21]
-    (load_sem, tp_send, tp_recv, x_send, x_recv, ep_send, ep_recv, here) = refs[21:]
+    (dout, xb, rsum_out, rsum_in, eout, einto) = refs[11:17]
+    (load_sem, tp_send, tp_recv, x_send, x_recv, ep_send, ep_recv, here) = refs[17:]
     ep = lax.axis_index("ep")
     t = lax.axis_index("tp")
     tp, own, group, heads = s.tp, s.own, s.group, s.heads
@@ -372,7 +372,7 @@
     slots = s.experts // 2
     some = rows // 2
     neighbour = across["ep"]
-    a_next, b_next, a_prev, b_prev, a_pass, b_pass = [], [], [], [], [], []
+    a_next, b_next, a_prev, b_prev, a_far, b_far = [], [], [], [], [], []
     for p in range(2):
         at = pl.ds(p * slots, slots)
 
@@ -383,20 +383,13 @@
         b_next.append(round_x(1, t, 1, nxt))
         a_prev.append(round_x(2, t, 0, prv))
         b_prev.append(round_x(3, t, 1, prv))
-        a_pass.append(round_x(4, prv, 0, nxt))
-        b_pass.append(round_x(5, nxt, 1, prv))
+        a_far.append(round_x(4, t, 0, far))
+        b_far.append(round_x(5, t, 1, far))
 
     for p in range(2):
         messages(dout, slots - p, ep_send.at[0], ep_recv.at[p], neighbour).wait_recv()
-        a_next[p].start()
-        b_prev[p].start()
-        b_next[p].start()
-        a_prev[p].start()
-    for p in range(2):
-        a_next[p].wait_recv()
-        a_pass[p].start()
-        b_prev[p].wait_recv()
-        b_pass[p].start()
+        for copy in (a_far, b_far, a_next, b_prev, b_next, a_prev):
+            copy[p].start()
     loads["gate"].wait()
     loads["up"].wait()
     loads["down"].wait()
@@ -417,53 +410,29 @@
     def terms(act, i):
         return dot(act, down[:, pl.ds(pl.multiple_of(i * part, part), part)])
 
-    acts, pairs, sums = [], [], []
+    acts, sums = [], []
     for p in range(2):
-        b_next[p].wait_recv()
-        a_prev[p].wait_recv()
-        a_pass[p].wait_recv()
-        b_pass[p].wait_recv()
+        for copy in (a_next, b_next, a_prev, b_prev, a_far, b_far):
+            copy[p].wait_recv()
         act = hidden(p)
         acts.append(act)
-        hops = [
-            x_copy(12 * p + 6, r2o.at[p, 0], r2i.at[p, 0], nxt),
-            x_copy(12 * p + 7, r2o.at[p, 1], r2i.at[p, 1], prv),
-            x_copy(12 * p + 8, rdo.at[p, 0], rdi.at[p, 0], nxt),
-            x_copy(12 * p + 9, rdo.at[p, 1], rdi.at[p, 1], prv),
-            x_copy(12 * p + 10, rpo.at[p, 0], rpi.at[p, 0], nxt),
-            x_copy(12 * p + 11, rpo.at[p, 1], rpi.at[p, 1], prv),
-        ]
+        hops = []
+        for d, who in ((2, far), (1, nxt), (3, prv)):
+            hop = x_copy(12 * p + 5 + d, rsum_out.at[p, d - 1], rsum_in.at[p, d - 1], who)
+            rsum_out[p, d - 1] = terms(act, who).astype(BF16)
+            hop.start()
+            hops.append(hop)
         sums.append(hops)
-        v = terms(act, far)
-        r2o[p, 0] = v[:, :LANES].astype(BF16)
-        hops[0].start()
-        r2o[p, 1] = v[:, LANES:].astype(BF16)
-        hops[1].start()
-        vn = terms(act, nxt)
-        rdo[p, 0] = vn[:, LANES:].astype(BF16)
-        hops[2].start()
-        vp = terms(act, prv)
-        rdo[p, 1] = vp[:, :LANES].astype(BF16)
-        hops[3].start()
-        pairs.append((vn[:, :LANES], vp[:, LANES:]))
-    for p in range(2):
-        hops, (vn, vp) = sums[p], pairs[p]
-        hops[0].wait_recv()
-        rpo[p, 0] = (vn + r2i[p, 0].astype(F32)).astype(BF16)
-        hops[4].start()
-        hops[1].wait_recv()
-        rpo[p, 1] = (vp + r2i[p, 1].astype(F32)).astype(BF16)
-        hops[5].start()
     mine = [terms(act, t) for act in acts]
     for p in range(2):
         hops, v = sums[p], mine[p]
         at = pl.ds(p * slots, slots)
-        for i in (2, 3, 4, 5):
-            hops[i].wait_recv()
-        answer = v[:, :LANES] + rpi[p, 0].astype(F32) + rdi[p, 1].astype(F32)
-        eout[0, at] = answer.astype(BF16).reshape(slots, cap, LANES)
-        answer = v[:, LANES:] + rpi[p, 1].astype(F32) + rdi[p, 0].astype(F32)
-        eout[1, at] = answer.astype(BF16).reshape(slots, cap, LANES)
+        for hop in hops:
+            hop.wait_recv()
+        answer = v + sum(rsum_in[p, d].astype(F32) for d in range(3))
+        for half in range(2):
+            piece = answer[:, half * LANES : (half + 1) * LANES].astype(BF16)
+            eout[half, at] = piece.reshape(slots, cap, LANES)
         for i in range(p * mid, (p + 1) * mid):
             for j in range(s.nyc):
                 if i < nz - 1 or j < last:
@@ -573,7 +542,7 @@
             b(2, *by_expert),
             b(tp, 2, *by_expert),
         ]
-        + [b(2, 2, rows // 2, LANES)] * 6
+        + [b(2, 3, rows // 2, part)] * 2
         + [b(2, *by_expert)] * 2
         + [
             sem((1 + len(operands),)),
@@ -586,9 +555,9 @@
             pltpu.SemaphoreType.REGULAR((6,)),
         ],
         compiler_params=pltpu.CompilerParams(
-            collective_id=0, has_side_effects=True
+            collective_id=0, has_side_effects=True, vmem_limit_bytes=24*2**20
         ),
-    )(tok, *operands)
+    )(*[pltpu.with_memory_space_constraint(a, pltpu.HBM) for a in (tok, *operands)])
 
 
 def solution(mesh, nz=8, cap=2):

time: 64.7 us -> 61 us (0.943)
  Pallas kernels: 63.1 us -> 60.2 us
  local copies, waits for them, and re-layouts: 1.3 us -> 0.6 us
    pallas_call x1, Pallas kernels: 63.1 us -> 60.2 us  [layer(): pl.pallas_call(functools.partial(kernel, s), out_shape=jax.ShapeDtypeStru...]
    unnamed x1, local copies, waits for them, and re-layouts: 1.3 us -> 0.6 us
where the time goes in v5:
time: 61 us; the launch traced here: 60.8 us
  Pallas kernels  60.2 us (99%)
    pallas_call x1, Pallas kernels, layer(): pl.pallas_call(functools.partial(kernel, s), out_shape=jax.ShapeDtypeStru...  60.2 us

profile of v5, /device:TPU:1, one launch (start us, length us, event | category | flops | bytes accessed | tf_op | source)
XLA Modules:
  0.0 60.8 jit_solution(7546932518481034600)
XLA Ops:
  0.0 60.2 %shard_map.172 = bf16[16,256]{1,0:T(8,128)(2,1)S(1)} custom-call(bf16[32,128]{1,0:T(8,128)(2,1)} %bitcast.18, s32[1,16]{1,0:T(1,128)} %bitcast.23, f32[1,128]{1,0:T(1,128)} %constant.2.clone.refs_2_, s32[6,16]{1,0:T(8,128)} %bitcast.19, f32[6,16]{1,0:T(8,128)} %bitcast.20, f32[1,4]{1,0:T(1,128)} %bitcast.24, f32[1,128]{1,0:T(1,128)} %bitcast.25, ...), custom_call_target="tpu_custom_call" | custom-call | tf_op jit(solution)/shard_map/pallas_call | solution.py:524
  60.2 0.6 copy.21

commit v6 on v5

--- a/solution.py
+++ b/solution.py
@@ -16,6 +16,7 @@
 LANES = 128
 SMALL = ("lens", "freqs", "routes", "logits", "lams", "hgain", "gain1", "gain2")
 NAMES = SMALL + ("wq", "wk", "wv", "kc", "vc", "wo", "gate", "up", "down")
+PIECES = 4
 MESH = pl.DeviceIdType.MESH
 BF16 = jnp.bfloat16
 F32 = jnp.float32
@@ -343,7 +344,7 @@
     settled = normed(summed, 3, stats1, gain1)
 
     by_expert = (s.experts, cap, LANES)
-    mid, last = nz // 2, s.nyc - 1
+    mid, last = nz // PIECES, s.nyc - 1
     for half in range(2):
         v = dot(place[...], settled[:, half * LANES : (half + 1) * LANES]).astype(BF16)
         dout[half] = v.reshape(by_expert)
@@ -369,11 +370,11 @@
         sent.append(copy)
         return copy
 
-    slots = s.experts // 2
-    some = rows // 2
+    slots = s.experts // PIECES
+    some = rows // PIECES
     neighbour = across["ep"]
     a_next, b_next, a_prev, b_prev, a_far, b_far = [], [], [], [], [], []
-    for p in range(2):
+    for p in range(PIECES):
         at = pl.ds(p * slots, slots)
 
         def round_x(i, who, half, to, p=p, at=at):
@@ -386,8 +387,8 @@
         a_far.append(round_x(4, t, 0, far))
         b_far.append(round_x(5, t, 1, far))
 
-    for p in range(2):
-        messages(dout, slots - p, ep_send.at[0], ep_recv.at[p], neighbour).wait_recv()
+    for p in range(PIECES):
+        messages(dout, slots - (p == PIECES - 1), ep_send.at[0], ep_recv.at[p], neighbour).wait_recv()
         for copy in (a_far, b_far, a_next, b_prev, b_next, a_prev):
             copy[p].start()
     loads["gate"].wait()
@@ -411,7 +412,7 @@
         return dot(act, down[:, pl.ds(pl.multiple_of(i * part, part), part)])
 
     acts, sums = [], []
-    for p in range(2):
+    for p in range(PIECES):
         for copy in (a_next, b_next, a_prev, b_prev, a_far, b_far):
             copy[p].wait_recv()
         act = hidden(p)
@@ -424,7 +425,7 @@
             hops.append(hop)
         sums.append(hops)
     mine = [terms(act, t) for act in acts]
-    for p in range(2):
+    for p in range(PIECES):
         hops, v = sums[p], mine[p]
         at = pl.ds(p * slots, slots)
         for hop in hops:
@@ -438,10 +439,10 @@
                 if i < nz - 1 or j < last:
                     slot = i * s.nyc + tails[j]
                     other = origins[i] + tails[j]
-                    post(eout.at[:, slot], einto.at[:, ep], ep_send.at[1], ep_recv.at[2], other)
+                    post(eout.at[:, slot], einto.at[:, ep], ep_send.at[1], ep_recv.at[PIECES], other)
     for half in range(2):
         einto[half, ep] = eout[half, (nz - 1) * s.nyc + line]
-    messages(eout, s.experts - 1, ep_send.at[1], ep_recv.at[2], neighbour).wait_recv()
+    messages(eout, s.experts - 1, ep_send.at[1], ep_recv.at[PIECES], neighbour).wait_recv()
 
     def combined(half):
         three = dot(pick[...], einto[half].reshape(rows, LANES))
@@ -454,7 +455,7 @@
     for copy in sent:
         copy.wait_send()
     messages(dout, s.experts - 1, ep_send.at[0], ep_recv.at[0], neighbour).wait_send()
-    messages(eout, s.experts - 1, ep_send.at[1], ep_recv.at[2], neighbour).wait_send()
+    messages(eout, s.experts - 1, ep_send.at[1], ep_recv.at[PIECES], neighbour).wait_send()
 
 
 def layer(
@@ -542,16 +543,16 @@
             b(2, *by_expert),
             b(tp, 2, *by_expert),
         ]
-        + [b(2, 3, rows // 2, part)] * 2
+        + [b(PIECES, 3, rows // PIECES, part)] * 2
         + [b(2, *by_expert)] * 2
         + [
             sem((1 + len(operands),)),
             sem((5, tp - 1)),
             sem((5, tp - 1)),
-            sem((24,)),
-            sem((24,)),
+            sem((12 * PIECES,)),
+            sem((12 * PIECES,)),
             sem((2,)),
-            sem((3,)),
+            sem((PIECES + 1,)),
             pltpu.SemaphoreType.REGULAR((6,)),
         ],
         compiler_params=pltpu.CompilerParams(

time: 61 us -> 59.7 us (0.979)
  Pallas kernels: 60.2 us -> 59 us
    pallas_call x1, Pallas kernels: 60.2 us -> 59 us  [layer(): pl.pallas_call(functools.partial(kernel, s), out_shape=jax.ShapeDtypeStru...]
where the time goes in v6:
time: 59.7 us; the launch traced here: 59.6 us
  Pallas kernels  59 us (99%)
  local copies, waits for them, and re-layouts  0.6 us (1%)
    pallas_call x1, Pallas kernels, layer(): pl.pallas_call(functools.partial(kernel, s), out_shape=jax.ShapeDtypeStru...  59 us

profile of v6, /device:TPU:1, one launch (start us, length us, event | category | flops | bytes accessed | tf_op | source)
XLA Modules:
  0.0 59.6 jit_solution(9430070234180372496)
XLA Ops:
  0.0 59.0 %shard_map.172 = bf16[16,256]{1,0:T(8,128)(2,1)S(1)} custom-call(bf16[32,128]{1,0:T(8,128)(2,1)} %bitcast.18, s32[1,16]{1,0:T(1,128)} %bitcast.23, f32[1,128]{1,0:T(1,128)} %constant.2.clone.refs_2_, s32[6,16]{1,0:T(8,128)} %bitcast.19, f32[6,16]{1,0:T(8,128)} %bitcast.20, f32[1,4]{1,0:T(1,128)} %bitcast.24, f32[1,128]{1,0:T(1,128)} %bitcast.25, ...), custom_call_target="tpu_custom_call" | custom-call | tf_op jit(solution)/shard_map/pallas_call | solution.py:525
  59.0 0.6 %copy.21 = bf16[16,256]{1,0:T(8,128)(2,1)} copy(bf16[16,256]{1,0:T(8,128)(2,1)S(1)} %shard_map.172) | data formatting | bytes 16384

commit v7 on v6

--- a/solution.py
+++ b/solution.py
@@ -373,24 +373,13 @@
     slots = s.experts // PIECES
     some = rows // PIECES
     neighbour = across["ep"]
-    a_next, b_next, a_prev, b_prev, a_far, b_far = [], [], [], [], [], []
+    gathers = []
     for p in range(PIECES):
-        at = pl.ds(p * slots, slots)
-
-        def round_x(i, who, half, to, p=p, at=at):
-            return x_copy(12 * p + i, xb.at[who, half, at], xb.at[who, half, at], to)
-
-        a_next.append(round_x(0, t, 0, nxt))
-        b_next.append(round_x(1, t, 1, nxt))
-        a_prev.append(round_x(2, t, 0, prv))
-        b_prev.append(round_x(3, t, 1, prv))
-        a_far.append(round_x(4, t, 0, far))
-        b_far.append(round_x(5, t, 1, far))
-
-    for p in range(PIECES):
+        block = xb.at[t, :, pl.ds(p * slots, slots)]
+        gathers.append([x_copy(6 * p + i, block, block, to) for i, to in enumerate((far, nxt, prv))])
         messages(dout, slots - (p == PIECES - 1), ep_send.at[0], ep_recv.at[p], neighbour).wait_recv()
-        for copy in (a_far, b_far, a_next, b_prev, b_next, a_prev):
-            copy[p].start()
+        for copy in gathers[p]:
+            copy.start()
     loads["gate"].wait()
     loads["up"].wait()
     loads["down"].wait()
@@ -413,13 +402,13 @@
 
     acts, sums = [], []
     for p in range(PIECES):
-        for copy in (a_next, b_next, a_prev, b_prev, a_far, b_far):
-            copy[p].wait_recv()
+        for copy in gathers[p]:
+            copy.wait_recv()
         act = hidden(p)
         acts.append(act)
         hops = []
         for d, who in ((2, far), (1, nxt), (3, prv)):
-            hop = x_copy(12 * p + 5 + d, rsum_out.at[p, d - 1], rsum_in.at[p, d - 1], who)
+            hop = x_copy(6 * p + 2 + d, rsum_out.at[p, d - 1], rsum_in.at[p, d - 1], who)
             rsum_out[p, d - 1] = terms(act, who).astype(BF16)
             hop.start()
             hops.append(hop)
@@ -549,8 +538,8 @@
             sem((1 + len(operands),)),
             sem((5, tp - 1)),
             sem((5, tp - 1)),
-            sem((12 * PIECES,)),
-            sem((12 * PIECES,)),
+            sem((6 * PIECES,)),
+            sem((6 * PIECES,)),
             sem((2,)),
             sem((PIECES + 1,)),
             pltpu.SemaphoreType.REGULAR((6,)),

time: 59.7 us -> 59.3 us (level)
  no operation moved by 1% of the time
where the time goes in v7:
time: 59.3 us; the launch traced here: 59.1 us
  Pallas kernels  58.5 us (99%)
  local copies, waits for them, and re-layouts  0.6 us (1%)
    pallas_call x1, Pallas kernels, layer(): pl.pallas_call(functools.partial(kernel, s), out_shape=jax.ShapeDtypeStru...  58.5 us

profile of v7, /device:TPU:1, one launch (start us, length us, event | category | flops | bytes accessed | tf_op | source)
XLA Modules:
  0.0 59.1 jit_solution(8234659498455210550)
XLA Ops:
  0.0 58.5 %shard_map.172 = bf16[16,256]{1,0:T(8,128)(2,1)S(1)} custom-call(bf16[32,128]{1,0:T(8,128)(2,1)} %bitcast.18, s32[1,16]{1,0:T(1,128)} %bitcast.23, f32[1,128]{1,0:T(1,128)} %constant.2.clone.refs_2_, s32[6,16]{1,0:T(8,128)} %bitcast.19, f32[6,16]{1,0:T(8,128)} %bitcast.20, f32[1,4]{1,0:T(1,128)} %bitcast.24, f32[1,128]{1,0:T(1,128)} %bitcast.25, ...), custom_call_target="tpu_custom_call" | custom-call | tf_op jit(solution)/shard_map/pallas_call | solution.py:514
  58.5 0.6 %copy.21 = bf16[16,256]{1,0:T(8,128)(2,1)} copy(bf16[16,256]{1,0:T(8,128)(2,1)S(1)} %shard_map.172) | data formatting | bytes 16384
